TPU v7x, 32 devices: a whole 2x2x4 slice. The times are simulated.
32 devices in a mesh: sp: 8 (over z, y), tp: 4 (over x, core).
Axes of the slice: x: 2, y: 2, z: 4, core: 2. Of those that a mesh axis runs over, the one named last changes fastest.
Arguments:
- glu_value: bfloat16 [4096, 1024], P('sp', 'tp'), may hold values from -6 to 6
- glu_gate: bfloat16 [4096, 1024], P('sp', 'tp'), may hold values from -8 to 8
- conv_taps: bfloat16 [31, 1024], P(None, 'tp'), may hold values from -1 to 1
- norm_gain: float32 [1024], P('tp'), may hold values from 0.1 to 1.9
- out_weight: bfloat16 [2048, 1024], P(None, 'tp'), may hold values from -0.1875 to 0.1875
- norm_mean: float32 [4096], P('sp'), may hold values from -3 to 3
- norm_scale: float32 [4096], P('sp'), may hold values from 0.5 to 2
- out_grad: bfloat16 [4096, 2048], P('sp'), may hold values from -6 to 6
Outputs:
- value_grad: bfloat16 [4096, 1024], P('sp', 'tp')
- gate_grad: bfloat16 [4096, 1024], P('sp', 'tp')
- taps_grad: float32 [31, 1024], P(None, 'tp')
- gain_grad: float32 [1024], P('tp')
- weight_grad: float32 [2048, 1024], P('sp', 'tp')
All inputs are finite; a program needn't handle non-finite values.
Results may differ from a plain program's by a relative error of at most 0.0047.
Values may be sent and summed in bfloat16 or wider, within the bound.
A program may use at most 64 MiB of HBM per device.

v0:
```python
import functools

import jax
import jax.numpy as jnp
from jax import lax
from jax.experimental import pallas as pl
from jax.experimental.pallas import tpu as pltpu
from jax.sharding import PartitionSpec as P

MESH = pl.DeviceIdType.MESH
F32 = jnp.float32
BF16 = jnp.bfloat16
LANES = 128
VMEM_LIMIT = 62 * 1024 * 1024
BLOCK = 64


def rup(value, unit):
    return -(-value // unit) * unit


def kernel(
    n, m, kw,
    val, gate, taps_in, gain, mean_row, scale_row, og_hbm, ow_hbm,
    value_grad, gate_grad, taps_out, gain_out, w_out,
    taps, og, ow, gp, sh, cg, sh2, centered, slope, act, agrad, psum, csum, meanb, scaleb,
    mpb, mcb, halo_out, halo_in, stats, taploc, tapin, tapsum, wsum, wbf, recv1, send2, recv2,
    load_sem, halo_sem, back_sem, stat_send, stat_recv, tap_send, tap_recv, all_send, all_recv,
    y_send, y_recv, z_send, z_recv,
):
    rows, chans = val.shape
    tiles = chans // LANES
    depth = og.shape[1]
    dr = depth // n
    half = n // 2
    reach = kw - 1
    halo = halo_out.shape[0]
    lead = halo - reach
    blocks = rows // BLOCK
    sp = lax.axis_index("sp")
    tp = lax.axis_index("tp")
    par = lax.rem(sp, 2)
    q = lax.div(sp, 2)
    partner = sp + 1 - 2 * par

    load_og = pltpu.make_async_copy(og_hbm, og, load_sem.at[0])
    load_ow = pltpu.make_async_copy(ow_hbm, ow, load_sem.at[1])
    load_og.start()
    load_ow.start()

    barrier = pltpu.get_barrier_semaphore()

    @pl.loop(1, n)
    def _(k):
        pl.semaphore_signal(
            barrier, inc=1, device_id={"sp": lax.rem(sp + k, n)}, device_id_type=MESH
        )

    @pl.loop(1, m)
    def _(k):
        pl.semaphore_signal(
            barrier, inc=1, device_id={"tp": lax.rem(tp + k, m)}, device_id_type=MESH
        )

    def lanes(ct):
        return slice(ct * LANES, (ct + 1) * LANES)

    taps[...] = taps_in[...].astype(F32)
    tail = slice(rows - halo, rows)
    tail_sig = jax.nn.sigmoid(gate[tail, :].astype(F32))
    halo_out[...] = (val[tail, :].astype(F32) * tail_sig).astype(BF16)

    def gate_block(b, _):
        at = pl.ds(pl.multiple_of(b * BLOCK, BLOCK), BLOCK)
        to = pl.ds(pl.multiple_of(b * BLOCK + halo, 16), BLOCK)
        for ct in range(tiles):
            sig = jax.nn.sigmoid(gate[at, lanes(ct)].astype(F32))
            gp[ct, to, :] = (val[at, lanes(ct)].astype(F32) * sig).astype(BF16).astype(F32)
        return 0

    lax.fori_loop(0, blocks, gate_block, 0)

    load_og.wait()
    load_ow.wait()
    slab = min(rows, 128)

    def grad_block(b, _):
        at = pl.ds(pl.multiple_of(b * slab, slab), slab)
        agrad[at, :] = jnp.dot(og[at, :], ow[...], preferred_element_type=F32)
        return 0

    lax.fori_loop(0, rows // slab, grad_block, 0)

    pl.semaphore_wait(barrier, n - 1 + m - 1)

    halo_copy = pltpu.make_async_remote_copy(
        src_ref=halo_out, dst_ref=halo_in,
        send_sem=halo_sem.at[0], recv_sem=halo_sem.at[1],
        device_id={"sp": lax.rem(sp + 1, n)}, device_id_type=MESH,
    )

    @pl.when(sp < n - 1)
    def _():
        halo_copy.start()

    def shifted(src, dst, begin, count):
        for ct in range(tiles):
            for r in range(1, 8):
                dst[r - 1, ct, begin : begin + count, :] = src[ct, begin + r : begin + r + count, :]

    for at in range(halo, rows + halo - 8, BLOCK):
        shifted(gp, sh, at, min(BLOCK, rows + halo - 8 - at))
    meanb[...] = jnp.broadcast_to(mean_row[...], (LANES, rows)).T
    scaleb[...] = jnp.broadcast_to(scale_row[...], (LANES, rows)).T

    def source(base_ref, copies, shift, ct, start, count):
        r, base = shift % 8, shift - shift % 8
        at = pl.ds(pl.multiple_of(start + base, 8), count)
        if r == 0:
            return base_ref[ct, at, :]
        return copies[r - 1, ct, at, :]

    def conv_block(b, _):
        start = pl.multiple_of(b * BLOCK, BLOCK)
        at = pl.ds(start, BLOCK)
        for ct in range(tiles):
            conv = jnp.zeros((BLOCK, LANES), F32)
            for k in range(kw):
                conv = conv + taps[k : k + 1, lanes(ct)] * source(gp, sh, k + lead, ct, start, BLOCK)
            cen = (conv - meanb[at, :]) * scaleb[at, :]
            nor = cen * gain[:, lanes(ct)]
            sig = jax.nn.sigmoid(nor)
            centered[ct, at, :] = cen
            slope[ct, at, :] = sig * (1.0 + nor * (1.0 - sig))
            act[at, lanes(ct)] = (nor * sig).astype(BF16)
        return 0

    lax.fori_loop(1, blocks, conv_block, 0)

    @pl.when(sp > 0)
    def _():
        halo_copy.wait_recv()
        for ct in range(tiles):
            gp[ct, 0:halo, :] = halo_in[:, lanes(ct)].astype(F32)

    @pl.when(sp == 0)
    def _():
        for ct in range(tiles):
            gp[ct, 0:halo, :] = jnp.zeros((halo, LANES), F32)

    shifted(gp, sh, 0, halo)
    conv_block(0, 0)

    wide = max(dr, min(depth, 256))

    def w_tile(start):
        start = pl.multiple_of(start, wide)
        part = lax.dot_general(
            og[:, pl.ds(start, wide)], act[...], (((0,), (0,)), ((), ())),
            preferred_element_type=F32,
        )
        wsum[pl.ds(start, wide), :] = part
        wbf[pl.ds(start, wide), :] = part.astype(BF16)

    def own_rows(p, side):
        return pl.ds(pl.multiple_of((2 * p + side) * dr, dr), dr)

    def y_copy(p):
        return pltpu.make_async_remote_copy(
            src_ref=wbf.at[own_rows(p, 1 - par), :], dst_ref=recv1.at[p],
            send_sem=y_send.at[p], recv_sem=y_recv.at[p],
            device_id={"sp": partner}, device_id_type=MESH,
        )

    def partner_step(k, _):
        p = lax.rem(q + k, half)
        w_tile((2 * p + 1 - par) * dr)
        y_copy(p).start()
        return 0

    def own_step(k, _):
        w_tile((2 * lax.rem(q + k, half) + par) * dr)
        return 0

    if wide == dr:
        lax.fori_loop(1, half, partner_step, 0)
        w_tile((2 * q + 1 - par) * dr)
    else:
        def tile_step(j, _):
            w_tile(j * wide)
            return 0

        lax.fori_loop(0, depth // wide, tile_step, 0)

        def send_step(k, _):
            y_copy(lax.rem(q + k, half)).start()
            return 0

        lax.fori_loop(1, half, send_step, 0)

    def stat_block(b, sums):
        at = pl.ds(pl.multiple_of(b * BLOCK, BLOCK), BLOCK)
        plain = jnp.zeros((BLOCK, LANES), F32)
        cross = jnp.zeros((BLOCK, LANES), F32)
        new = []
        for ct in range(tiles):
            cen = centered[ct, at, :]
            ngrad = agrad[at, lanes(ct)] * slope[ct, at, :]
            scaled = ngrad * gain[:, lanes(ct)]
            agrad[at, lanes(ct)] = scaled
            plain = plain + scaled
            cross = cross + scaled * cen
            new.append(sums[ct] + jnp.sum((ngrad * cen).reshape(BLOCK // 8, 8, LANES), axis=0))
        psum[at, :] = plain
        csum[at, :] = cross
        return tuple(new)

    gains = lax.fori_loop(
        0, blocks, stat_block, tuple(jnp.zeros((8, LANES), F32) for _ in range(tiles))
    )
    stats[tp, 0:1, :] = jnp.sum(psum[...].T, axis=0, keepdims=True)
    stats[tp, 1:2, :] = jnp.sum(csum[...].T, axis=0, keepdims=True)

    def stat_copy(k, slot):
        return pltpu.make_async_remote_copy(
            src_ref=stats.at[slot], dst_ref=stats.at[slot],
            send_sem=stat_send.at[k], recv_sem=stat_recv.at[slot],
            device_id={"tp": lax.rem(tp + k, m)}, device_id_type=MESH,
        )

    @pl.loop(1, m)
    def _(k):
        stat_copy(k, tp).start()

    if wide == dr:
        lax.fori_loop(1, half + 1, own_step, 0)

    share = taploc.shape[2]

    def keep_tap(k, ct, sums):
        taploc[k // share, ct, k % share : k % share + 1, :] = jnp.sum(sums, axis=0, keepdims=True)

    for ct in range(tiles):
        keep_tap(kw, ct, gains[ct])
        for k in range(kw + 1, n * share):
            keep_tap(k, ct, jnp.zeros((8, LANES), F32))

    @pl.loop(1, m)
    def _(k):
        stat_copy(k, lax.rem(tp + m - k, m)).wait_recv()

    totals = stats[0]
    for k in range(1, m):
        totals = totals + stats[k]
    totals = totals / (chans * m)
    mpb[...] = jnp.broadcast_to(totals[0:1, :], (LANES, rows)).T
    mcb[...] = jnp.broadcast_to(totals[1:2, :], (LANES, rows)).T

    def cg_block(b, _):
        at = pl.ds(pl.multiple_of(b * BLOCK, BLOCK), BLOCK)
        for ct in range(tiles):
            cg[ct, at, :] = scaleb[at, :] * (
                agrad[at, lanes(ct)] - mpb[at, :] - centered[ct, at, :] * mcb[at, :]
            )
        return 0

    lax.fori_loop(0, blocks, cg_block, 0)
    back_copy = pltpu.make_async_remote_copy(
        src_ref=cg.at[:, pl.ds(0, halo), :], dst_ref=cg.at[:, pl.ds(rows, halo), :],
        send_sem=back_sem.at[0], recv_sem=back_sem.at[1],
        device_id={"sp": lax.rem(sp + n - 1, n)}, device_id_type=MESH,
    )

    @pl.when(sp > 0)
    def _():
        back_copy.start()

    def z_copy(k, p, slot):
        return pltpu.make_async_remote_copy(
            src_ref=send2.at[p], dst_ref=recv2.at[slot],
            send_sem=z_send.at[k], recv_sem=z_recv.at[slot],
            device_id={"sp": 2 * p + par}, device_id_type=MESH,
        )

    def relay(k, _):
        p = lax.rem(q + k, half)
        y_copy(p).wait_recv()
        send2[p] = (wsum[own_rows(p, par), :] + recv1[p].astype(F32)).astype(BF16)
        z_copy(k, p, q).start()
        return 0

    cut1 = 1 + (half - 1 + 2) // 3
    cut2 = cut1 + (half - cut1 + 1) // 2
    lax.fori_loop(1, cut1, relay, 0)

    span = 16
    for ct in range(tiles):
        def tap_block(b, sums, ct=ct):
            start = pl.multiple_of(b * span, span)
            grad = cg[ct, pl.ds(start, span), :]
            new = []
            for k in range(kw):
                prod = grad * source(gp, sh, k + lead, ct, start, span)
                new.append(sums[k] + jnp.sum(prod.reshape(span // 8, 8, LANES), axis=0))
            return tuple(new)

        sums = lax.fori_loop(
            0, rows // span, tap_block, tuple(jnp.zeros((8, LANES), F32) for _ in range(kw))
        )
        for k in range(kw):
            keep_tap(k, ct, sums[k])

    def tap_copy(k, slot):
        peer = lax.rem(sp + k, n)
        return pltpu.make_async_remote_copy(
            src_ref=taploc.at[peer], dst_ref=tapin.at[slot],
            send_sem=tap_send.at[k], recv_sem=tap_recv.at[slot],
            device_id={"sp": peer}, device_id_type=MESH,
        )

    def all_copy(k, slot):
        return pltpu.make_async_remote_copy(
            src_ref=tapsum.at[slot], dst_ref=tapsum.at[slot],
            send_sem=all_send.at[k], recv_sem=all_recv.at[slot],
            device_id={"sp": lax.rem(sp + k, n)}, device_id_type=MESH,
        )

    @pl.loop(1, n)
    def _(k):
        tap_copy(k, sp).start()

    y_copy(q).start()

    lax.fori_loop(cut1, cut2, relay, 0)

    for at in range(0, rows - 8, BLOCK):
        shifted(cg, sh2, at, min(BLOCK, rows - 8 - at))

    def back_block(b, _):
        start = pl.multiple_of(b * BLOCK, BLOCK)
        at = pl.ds(start, BLOCK)
        for ct in range(tiles):
            total = jnp.zeros((BLOCK, LANES), F32)
            for k in range(kw):
                total = total + taps[k : k + 1, lanes(ct)] * source(
                    cg, sh2, reach - k, ct, start, BLOCK
                )
            sig = jax.nn.sigmoid(gate[at, lanes(ct)].astype(F32))
            value_grad[at, lanes(ct)] = (total * sig).astype(BF16)
            gate_grad[at, lanes(ct)] = (
                total * val[at, lanes(ct)].astype(F32) * sig * (1.0 - sig)
            ).astype(BF16)
        return 0

    lax.fori_loop(0, blocks - 1, back_block, 0)

    @pl.when(sp < n - 1)
    def _():
        back_copy.wait_recv()

    @pl.when(sp == n - 1)
    def _():
        cg[:, rows : rows + halo, :] = jnp.zeros((tiles, halo, LANES), F32)

    shifted(cg, sh2, rows - 8, halo)
    back_block(blocks - 1, 0)

    lax.fori_loop(cut2, half, relay, 0)

    def tap_wait(k, total):
        slot = lax.rem(sp + n - k, n)
        tap_copy(k, slot).wait_recv()
        return total + tapin[slot]

    tapsum[sp] = lax.fori_loop(1, n, tap_wait, taploc[sp])

    @pl.loop(1, n)
    def _(k):
        all_copy(k, sp).start()

    y_copy(q).wait_recv()
    w_out[...] = wsum[own_rows(q, par), :] + recv1[q].astype(F32)

    def z_wait(k, _):
        p = lax.rem(q + half - k, half)
        z_copy(k, p, p).wait_recv()
        w_out[...] += recv2[p].astype(F32)
        return 0

    lax.fori_loop(1, half, z_wait, 0)

    @pl.loop(1, n)
    def _(k):
        all_copy(k, lax.rem(sp + n - k, n)).wait_recv()

    for ct in range(tiles):
        for k in range(kw):
            taps_out[k : k + 1, lanes(ct)] = tapsum[k // share, ct, k % share : k % share + 1, :]
        gain_out[:, lanes(ct)] = tapsum[kw // share, ct, kw % share : kw % share + 1, :]

    @pl.when(sp < n - 1)
    def _():
        halo_copy.wait_send()

    @pl.when(sp > 0)
    def _():
        back_copy.wait_send()

    @pl.loop(1, m)
    def _(k):
        stat_copy(k, tp).wait_send()

    @pl.loop(1, n)
    def _(k):
        tap_copy(k, sp).wait_send()
        all_copy(k, sp).wait_send()

    @pl.loop(0, half)
    def _(k):
        y_copy(k).wait_send()

    @pl.loop(1, half)
    def _(k):
        z_copy(k, lax.rem(q + k, half), q).wait_send()


def finish(count, *refs):
    for source, target in zip(refs[:count], refs[count:]):
        target[...] = source[...]


def per_device(
    n, m, glu_value, glu_gate, conv_taps, norm_gain, out_weight, norm_mean, norm_scale, out_grad
):
    rows, chans = glu_value.shape
    kw = conv_taps.shape[0]
    depth = out_grad.shape[1]
    dr = depth // n
    half = n // 2
    tiles = chans // LANES
    halo = rup(kw - 1, 16)
    vm = pltpu.VMEM
    dma = pltpu.SemaphoreType.DMA
    whole = pl.BlockSpec(memory_space=pltpu.VMEM)
    far = pl.BlockSpec(memory_space=pltpu.HBM)
    out = pl.pallas_call(
        functools.partial(kernel, n, m, kw),
        out_shape=(
            jax.ShapeDtypeStruct((rows, chans), BF16),
            jax.ShapeDtypeStruct((rows, chans), BF16),
            jax.ShapeDtypeStruct((kw, chans), F32),
            jax.ShapeDtypeStruct((1, chans), F32),
            jax.ShapeDtypeStruct((dr, chans), F32),
        ),
        in_specs=[whole] * 6 + [far] * 2,
        out_specs=(whole,) * 5,
        scratch_shapes=[
            vm((kw, chans), F32),
            vm((rows, depth), BF16),
            vm((depth, chans), BF16),
            vm((tiles, rows + halo, LANES), F32),
            vm((7, tiles, rows + halo, LANES), F32),
            vm((tiles, rows + halo, LANES), F32),
            vm((7, tiles, rows + halo, LANES), F32),
            vm((tiles, rows, LANES), F32),
            vm((tiles, rows, LANES), F32),
            vm((rows, chans), BF16),
            vm((rows, chans), F32),
            vm((rows, LANES), F32),
            vm((rows, LANES), F32),
            vm((rows, LANES), F32),
            vm((rows, LANES), F32),
            vm((rows, LANES), F32),
            vm((rows, LANES), F32),
            vm((halo, chans), BF16),
            vm((halo, chans), BF16),
            vm((m, 2, rows), F32),
            vm((n, tiles, rup(kw + 1, n) // n, LANES), F32),
            vm((n, tiles, rup(kw + 1, n) // n, LANES), F32),
            vm((n, tiles, rup(kw + 1, n) // n, LANES), F32),
            vm((depth, chans), F32),
            vm((depth, chans), BF16),
            vm((half, dr, chans), BF16),
            vm((half, dr, chans), BF16),
            vm((half, dr, chans), BF16),
            dma((2,)), dma((2,)), dma((2,)),
            dma((m,)), dma((m,)), dma((n,)), dma((n,)), dma((n,)), dma((n,)),
            dma((half,)), dma((half,)), dma((half,)), dma((half,)),
        ],
        compiler_params=pltpu.CompilerParams(
            collective_id=0, has_side_effects=True, vmem_limit_bytes=VMEM_LIMIT
        ),
    )(
        glu_value, glu_gate, conv_taps, norm_gain[None, :],
        norm_mean[None, :], norm_scale[None, :], out_grad, out_weight,
    )
    out = pl.pallas_call(
        functools.partial(finish, len(out)),
        out_shape=tuple(jax.ShapeDtypeStruct(x.shape, x.dtype) for x in out),
        in_specs=[whole] * len(out),
        out_specs=(whole,) * len(out),
        compiler_params=pltpu.CompilerParams(vmem_limit_bytes=VMEM_LIMIT),
    )(*out)
    value_grad, gate_grad, taps_grad, gain_grad, weight_grad = out
    return value_grad, gate_grad, taps_grad, gain_grad[0], weight_grad


def solution(mesh):
    placed = (
        P("sp", "tp"), P("sp", "tp"), P(None, "tp"), P("tp"),
        P(None, "tp"), P("sp"), P("sp"), P("sp", None),
    )
    return jax.shard_map(
        functools.partial(per_device, mesh.shape["sp"], mesh.shape["tp"]),
        mesh=mesh,
        in_specs=placed,
        out_specs=(P("sp", "tp"), P("sp", "tp"), P(None, "tp"), P("tp"), P("sp", "tp")),
        check_vma=False,
    )
```

profile of v0, /device:TPU:0, one launch (start us, length us, event | category | flops | bytes accessed | tf_op | source)
XLA Modules:
  0.0 36.4 jit_solution(18368438383210273396)
XLA Ops:
  0.6 33.7 %shard_map.119 = (bf16[512,256]{1,0:T(8,128)(2,1)}, bf16[512,256]{1,0:T(8,128)(2,1)}, f32[31,256]{1,0:T(8,128)}, f32[1,256]{1,0:T(1,128)}, f32[256,256]{1,0:T(8,128)}) custom-call(bf16[512,256]{1,0:T(8,128)(2,1)} %val.1, bf16[512,256]{1,0:T(8,128)(2,1)} %gate.1, bf16[31,256]{1,0:T(8,128)(2,1)} %taps_in.1, f32[1,256]{1,0:T(1,128)} %bitcast.6, ...), custom_call_target="tpu_custom_call" | custom-call | tf_op jit(solution)/shard_map/pallas_call | solution.py:446
  34.3 2.0 %shard_map.120 = (bf16[512,256]{1,0:T(8,128)(2,1)}, bf16[512,256]{1,0:T(8,128)(2,1)}, f32[31,256]{1,0:T(8,128)}, f32[1,256]{1,0:T(1,128)}, f32[256,256]{1,0:T(8,128)}) custom-call(bf16[512,256]{1,0:T(8,128)(2,1)} %get-tuple-element.15.refs_0_, bf16[512,256]{1,0:T(8,128)(2,1)} %get-tuple-element.16.refs_1_, f32[31,256]{1,0:T(8,128)} %get-tuple-element.17.refs_2_, ...), custom_call_target="tpu_custom_call" | custom-call | tf_op jit(solution)/shard_map/pallas_call | solution.py:497
where the time goes:
time: 36.5 us; the launch traced here: 36.4 us
  Pallas kernels  35.7 us (98%)
  between operations  0.64 us (2%)
    pallas_call x1, Pallas kernels, per_device(): pl.pallas_call(functools.partial(kernel, n, m, kw), out_shape=(jax.ShapeD...  33.7 us
    pallas_call x1, Pallas kernels, per_device(): pl.pallas_call(functools.partial(finish, len(out)), out_shape=tuple((jax....  2.04 us

commit v1 on v0

--- a/solution.py
+++ b/solution.py
@@ -11,7 +11,7 @@
 F32 = jnp.float32
 BF16 = jnp.bfloat16
 LANES = 128
-VMEM_LIMIT = 62 * 1024 * 1024
+VMEM_LIMIT = 30 * 1024 * 1024
 BLOCK = 64
 
 
@@ -425,8 +425,15 @@
 
 
 def finish(count, *refs):
-    for source, target in zip(refs[:count], refs[count:]):
-        target[...] = source[...]
+    sem = refs[-1]
+    copies = [
+        pltpu.make_async_copy(source, target, sem.at[k])
+        for k, (source, target) in enumerate(zip(refs[:count], refs[count : 2 * count]))
+    ]
+    for copy in copies:
+        copy.start()
+    for copy in copies:
+        copy.wait()
 
 
 def per_device(
@@ -446,11 +453,11 @@
     out = pl.pallas_call(
         functools.partial(kernel, n, m, kw),
         out_shape=(
-            jax.ShapeDtypeStruct((rows, chans), BF16),
-            jax.ShapeDtypeStruct((rows, chans), BF16),
-            jax.ShapeDtypeStruct((kw, chans), F32),
-            jax.ShapeDtypeStruct((1, chans), F32),
-            jax.ShapeDtypeStruct((dr, chans), F32),
+            pltpu.VMEM((rows, chans), BF16),
+            pltpu.VMEM((rows, chans), BF16),
+            pltpu.VMEM((kw, chans), F32),
+            pltpu.VMEM((1, chans), F32),
+            pltpu.VMEM((dr, chans), F32),
         ),
         in_specs=[whole] * 6 + [far] * 2,
         out_specs=(whole,) * 5,
@@ -490,16 +497,18 @@
         compiler_params=pltpu.CompilerParams(
             collective_id=0, has_side_effects=True, vmem_limit_bytes=VMEM_LIMIT
         ),
-    )(
+    )(*[
+        pltpu.with_memory_space_constraint(x, pltpu.HBM) for x in (
         glu_value, glu_gate, conv_taps, norm_gain[None, :],
         norm_mean[None, :], norm_scale[None, :], out_grad, out_weight,
-    )
+    )])
     out = pl.pallas_call(
         functools.partial(finish, len(out)),
         out_shape=tuple(jax.ShapeDtypeStruct(x.shape, x.dtype) for x in out),
         in_specs=[whole] * len(out),
-        out_specs=(whole,) * len(out),
-        compiler_params=pltpu.CompilerParams(vmem_limit_bytes=VMEM_LIMIT),
+        out_specs=(pl.BlockSpec(memory_space=pltpu.HBM),) * len(out),
+        scratch_shapes=[pltpu.SemaphoreType.DMA((len(out),))],
+        compiler_params=pltpu.CompilerParams(vmem_limit_bytes=2 * 1024 * 1024),
     )(*out)
     value_grad, gate_grad, taps_grad, gain_grad, weight_grad = out
     return value_grad, gate_grad, taps_grad, gain_grad[0], weight_grad

time: 36.5 us -> 34.5 us (0.945)
  Pallas kernels: 35.7 us -> 33.7 us
    pallas_call x1, Pallas kernels: 2.04 us -> 0.94 us  [per_device(): pl.pallas_call(functools.partial(finish, len(out)), out_shape=tuple((jax....]
    pallas_call x1, Pallas kernels: 33.7 us -> 32.8 us  [per_device(): pl.pallas_call(functools.partial(kernel, n, m, kw), out_shape=(pltpu.VMEM...]
where the time goes in v1:
time: 34.5 us; the launch traced here: 34.4 us
  Pallas kernels  33.7 us (98%)
  between operations  0.64 us (2%)
    pallas_call x1, Pallas kernels, per_device(): pl.pallas_call(functools.partial(kernel, n, m, kw), out_shape=(pltpu.VMEM...  32.8 us
    pallas_call x1, Pallas kernels, per_device(): pl.pallas_call(functools.partial(finish, len(out)), out_shape=tuple((jax....  0.94 us

profile of v1, /device:TPU:0, one launch (start us, length us, event | category | flops | bytes accessed | tf_op | source)
XLA Modules:
  0.0 34.4 jit_solution(7676993516550295800)
XLA Ops:
  0.6 32.8 %shard_map.119 = (bf16[512,256]{1,0:T(8,128)(2,1)S(1)}, bf16[512,256]{1,0:T(8,128)(2,1)S(1)}, f32[31,256]{1,0:T(8,128)S(1)}, f32[1,256]{1,0:T(1,128)S(1)}, f32[256,256]{1,0:T(8,128)S(1)}) custom-call(bf16[512,256]{1,0:T(8,128)(2,1)} %val.1, bf16[512,256]{1,0:T(8,128)(2,1)} %gate.1, bf16[31,256]{1,0:T(8,128)(2,1)} %taps_in.1, f32[1,256]{1,0:T(1,128)} %bitcast.6, ...), custom_call_target="tpu_custom_call" | custom-call | tf_op jit(solution)/shard_map/pallas_call | solution.py:453
  33.4 0.9 %shard_map.120 = (bf16[512,256]{1,0:T(8,128)(2,1)}, bf16[512,256]{1,0:T(8,128)(2,1)}, f32[31,256]{1,0:T(8,128)}, f32[1,256]{1,0:T(1,128)}, f32[256,256]{1,0:T(8,128)}) custom-call(bf16[512,256]{1,0:T(8,128)(2,1)S(1)} %get-tuple-element.15.refs_0_, bf16[512,256]{1,0:T(8,128)(2,1)S(1)} %get-tuple-element.16.refs_1_, f32[31,256]{1,0:T(8,128)S(1)} %get-tuple-element.17.refs_2_, ...), custom_call_target="tpu_custom_call" | custom-call | tf_op jit(solution)/shard_map/pallas_call | solution.py:505

commit v2 on v1

--- a/solution.py
+++ b/solution.py
@@ -424,6 +424,549 @@
         z_copy(k, lax.rem(q + k, half), q).wait_send()
 
 
+def pair_kernel(
+    n, m, kw,
+    val_hbm, gate_hbm, taps_hbm, gain_hbm, mean_hbm, scale_hbm, og_hbm, ow_hbm,
+    value_grad, gate_grad, taps_out, gain_out, w_out,
+    val, gate, taps_in, gain, mean_row, scale_row, og, ow,
+    taps, gp, cg, centered, slope, act, actt, agrad, psum, csum, meanb, scaleb, mpb, mcb,
+    halo_out, halo_in, stats, taploc, tappair, tapz, wsum, ysend, yrecv, zsend, zrecv, xrecv,
+    zfown, zfsend, zfside, zfx, zfysend, zfyrecv, whole,
+    load_sem, halo_sem, back_sem, stat_send, stat_recv, pair_sem, tap_send, tap_recv,
+    y_send, y_recv, z_send, z_recv, x_recv, zf_send, zf_recv, zfy_sem, hop,
+):
+    rows, chans = val.shape
+    tiles = chans // LANES
+    depth = og.shape[1]
+    dr = depth // n
+    half = n // 2
+    reach = kw - 1
+    halo = halo_out.shape[0]
+    lead = halo - reach
+    blocks = rows // BLOCK
+    zf = chans // 4
+    cut = (chans - zf) // 2
+    sp = lax.axis_index("sp")
+    tp = lax.axis_index("tp")
+    par = lax.rem(sp, 2)
+    q = lax.div(sp, 2)
+    partner = sp + 1 - 2 * par
+    low = q < 2
+    outer = jnp.logical_or(q == 0, q == 3)
+    sib = q + 1 - 2 * lax.rem(q, 2)
+
+    barrier = pltpu.get_barrier_semaphore()
+
+    up, down = q < half - 1, q > 0
+    skew = jnp.where(par == 1, sp + 1, sp - 1)
+    has_skew = jnp.logical_and(skew >= 0, skew < n)
+
+    def greet(other):
+        pl.semaphore_signal(barrier, inc=1, device_id={"sp": other}, device_id_type=MESH)
+
+    greet(partner)
+
+    @pl.when(up)
+    def _():
+        greet(sp + 2)
+
+    @pl.when(down)
+    def _():
+        greet(sp - 2)
+
+    @pl.when(has_skew)
+    def _():
+        greet(skew)
+
+    @pl.loop(1, m)
+    def _(k):
+        pl.semaphore_signal(
+            barrier, inc=1, device_id={"tp": lax.rem(tp + k, m)}, device_id_type=MESH
+        )
+
+    loads = [
+        pltpu.make_async_copy(source, target, load_sem.at[k])
+        for k, (source, target) in enumerate((
+            (gate_hbm, gate), (val_hbm, val), (taps_hbm, taps_in), (mean_hbm, mean_row),
+            (scale_hbm, scale_row), (gain_hbm, gain), (og_hbm, og), (ow_hbm, ow),
+        ))
+    ]
+    for load in loads:
+        load.start()
+
+    def lanes(ct):
+        return slice(ct * LANES, (ct + 1) * LANES)
+
+    for load in loads[:6]:
+        load.wait()
+    tail = slice(rows - halo, rows)
+    tail_sig = jax.nn.sigmoid(gate[tail, :].astype(F32))
+    halo_out[...] = (val[tail, :].astype(F32) * tail_sig).astype(BF16)
+    taps[...] = taps_in[...].astype(F32)
+
+    def gate_block(b, _):
+        at = pl.ds(pl.multiple_of(b * BLOCK, BLOCK), BLOCK)
+        to = pl.ds(pl.multiple_of(b * BLOCK + halo, 16), BLOCK)
+        for ct in range(tiles):
+            sig = jax.nn.sigmoid(gate[at, lanes(ct)].astype(F32))
+            gp[ct, to, :] = (val[at, lanes(ct)].astype(F32) * sig).astype(BF16).astype(F32)
+        return 0
+
+    lax.fori_loop(0, blocks, gate_block, 0)
+    near = up.astype(jnp.int32) + down.astype(jnp.int32) + has_skew.astype(jnp.int32)
+    pl.semaphore_wait(barrier, m + near)
+
+    halo_copy = pltpu.make_async_remote_copy(
+        src_ref=halo_out, dst_ref=halo_in,
+        send_sem=halo_sem.at[0], recv_sem=halo_sem.at[1],
+        device_id={"sp": lax.rem(sp + 1, n)}, device_id_type=MESH,
+    )
+
+    @pl.when(sp < n - 1)
+    def _():
+        halo_copy.start()
+
+    def tell(r):
+        @pl.when(up)
+        def _():
+            pl.semaphore_signal(
+                hop.at[r, 0], inc=1, device_id={"sp": sp + 2}, device_id_type=MESH
+            )
+
+        @pl.when(down)
+        def _():
+            pl.semaphore_signal(
+                hop.at[r, 1], inc=1, device_id={"sp": sp - 2}, device_id_type=MESH
+            )
+
+    def hear(r):
+        @pl.when(down)
+        def _():
+            pl.semaphore_wait(hop.at[r, 0], 1)
+
+        @pl.when(up)
+        def _():
+            pl.semaphore_wait(hop.at[r, 1], 1)
+
+    tell(0)
+    meanb[...] = jnp.broadcast_to(mean_row[...], (LANES, rows)).T
+    scaleb[...] = jnp.broadcast_to(scale_row[...], (LANES, rows)).T
+    def source(ref, shift, ct, start, count):
+        return ref[ct, pl.ds(start + shift, count), :]
+
+    def conv_block(b, _):
+        start = pl.multiple_of(b * BLOCK, BLOCK)
+        at = pl.ds(start, BLOCK)
+        for ct in range(tiles):
+            conv = jnp.zeros((BLOCK, LANES), F32)
+            for k in range(kw):
+                conv = conv + taps[k : k + 1, lanes(ct)] * source(gp, k + lead, ct, start, BLOCK)
+            cen = (conv - meanb[at, :]) * scaleb[at, :]
+            nor = cen * gain[:, lanes(ct)]
+            sig = jax.nn.sigmoid(nor)
+            centered[ct, at, :] = cen
+            slope[ct, at, :] = sig * (1.0 + nor * (1.0 - sig))
+            act[at, lanes(ct)] = (nor * sig).astype(BF16)
+        return 0
+
+    def turn(chunk):
+        at = slice(chunk * LANES, (chunk + 1) * LANES)
+        for ct in range(tiles):
+            actt[lanes(ct), at] = act[at, lanes(ct)].T
+
+    lax.fori_loop(1, blocks, conv_block, 0)
+    for chunk in range(1, rows // LANES):
+        turn(chunk)
+
+    for load in loads[6:]:
+        load.wait()
+    slab = min(rows, 256)
+
+    def grad_block(b, _):
+        at = pl.ds(pl.multiple_of(b * slab, slab), slab)
+        agrad[at, :] = jnp.dot(og[at, :], ow[...], preferred_element_type=F32)
+        return 0
+
+    lax.fori_loop(0, rows // slab, grad_block, 0)
+
+    def stat_block(b, sums):
+        at = pl.ds(pl.multiple_of(b * BLOCK, BLOCK), BLOCK)
+        plain = jnp.zeros((BLOCK, LANES), F32)
+        cross = jnp.zeros((BLOCK, LANES), F32)
+        new = []
+        for ct in range(tiles):
+            cen = centered[ct, at, :]
+            ngrad = agrad[at, lanes(ct)] * slope[ct, at, :]
+            scaled = ngrad * gain[:, lanes(ct)]
+            agrad[at, lanes(ct)] = scaled
+            plain = plain + scaled
+            cross = cross + scaled * cen
+            new.append(sums[ct] + jnp.sum((ngrad * cen).reshape(BLOCK // 8, 8, LANES), axis=0))
+        psum[at, :] = plain
+        csum[at, :] = cross
+        return tuple(new)
+
+    gains = lax.fori_loop(
+        1, blocks, stat_block, tuple(jnp.zeros((8, LANES), F32) for _ in range(tiles))
+    )
+
+    hear(0)
+    tell(1)
+
+    @pl.when(sp > 0)
+    def _():
+        halo_copy.wait_recv()
+        for ct in range(tiles):
+            gp[ct, 0:halo, :] = halo_in[:, lanes(ct)].astype(F32)
+
+    @pl.when(sp == 0)
+    def _():
+        for ct in range(tiles):
+            gp[ct, 0:halo, :] = jnp.zeros((halo, LANES), F32)
+
+    conv_block(0, 0)
+    turn(0)
+    gains = stat_block(0, gains)
+    stats[tp, 0:1, :] = jnp.sum(psum[...].T, axis=0, keepdims=True)
+    stats[tp, 1:2, :] = jnp.sum(csum[...].T, axis=0, keepdims=True)
+
+    def stat_copy(k, slot):
+        return pltpu.make_async_remote_copy(
+            src_ref=stats.at[slot], dst_ref=stats.at[slot],
+            send_sem=stat_send.at[k], recv_sem=stat_recv.at[slot],
+            device_id={"tp": lax.rem(tp + k, m)}, device_id_type=MESH,
+        )
+
+    @pl.loop(1, m)
+    def _(k):
+        stat_copy(k, tp).start()
+
+    def piece(i):
+        far = (i, i - 1)
+        near_first = jnp.where(low, half - 1 - far[1], far[1]) if i else sib
+        far_first = jnp.where(low, half - 1 - far[0], far[0]) if i < 2 else sib
+        return jnp.where(outer, far_first, near_first)
+
+    order = [piece(0), piece(1), piece(2), q]
+    parts = (slice(0, cut), slice(cut, 2 * cut))
+    last = slice(2 * cut, chans)
+
+    def product(block):
+        at = pl.ds(pl.multiple_of(block * dr, LANES), dr)
+        return jnp.dot(actt[...], og[:, at], preferred_element_type=F32)
+
+    def y_copy(p, s):
+        return pltpu.make_async_remote_copy(
+            src_ref=ysend.at[p, s], dst_ref=yrecv.at[p, s],
+            send_sem=y_send.at[p, s], recv_sem=y_recv.at[p, s],
+            device_id={"sp": partner}, device_id_type=MESH,
+        )
+
+    def away(p):
+        part = product(2 * p + 1 - par)
+        for s in range(2):
+            ysend[p, s] = part[parts[s], :].astype(BF16)
+        zfown[p, 0] = part[last, :]
+
+    def home(p):
+        part = product(2 * p + par)
+        for s in range(2):
+            wsum[p, s] = part[parts[s], :]
+        zfown[p, 1] = part[last, :]
+
+    ahead = lax.rem(tp, 2) == 0
+
+    def send(cond, halves):
+        @pl.when(cond)
+        def _():
+            for i, s in halves:
+                y_copy(order[i], s).start()
+
+    def zf_copy(i, peer, target, sem):
+        return pltpu.make_async_remote_copy(
+            src_ref=zfsend.at[i], dst_ref=target,
+            send_sem=zf_send.at[i], recv_sem=sem,
+            device_id={"sp": 2 * peer + par}, device_id_type=MESH,
+        )
+
+    def zf_side(i, p):
+        return zf_copy(i, sib, zfside.at[p], zf_recv.at[p])
+
+    def zf_cross(i, p):
+        return zf_copy(i, p, zfx, x_recv.at[2])
+
+    def zf_first(i):
+        zfsend[i] = zfown[order[i]].astype(BF16)
+        zf_side(i, order[i]).start()
+
+    def zf_relay(i):
+        zf_side(0, order[i]).wait_recv()
+        zfsend[i] = (zfown[order[i]] + zfside[order[i]].astype(F32)).astype(BF16)
+        zf_cross(i, order[i]).start()
+
+    inner = jnp.logical_not(outer)
+    away(order[0])
+    send(ahead, ((0, 0), (0, 1)))
+    away(order[1])
+    send(ahead, ((1, 0), (1, 1)))
+    home(order[0])
+    zf_first(0)
+    home(order[1])
+
+    @pl.when(outer)
+    def _():
+        zf_first(1)
+
+    away(order[2])
+    home(order[2])
+
+    @pl.when(outer)
+    def _():
+        zf_first(2)
+
+    send(jnp.logical_not(ahead), ((0, 0), (0, 1)))
+    away(order[3])
+    home(order[3])
+
+    @pl.loop(1, m)
+    def _(k):
+        stat_copy(k, lax.rem(tp + m - k, m)).wait_recv()
+
+    totals = stats[0]
+    for k in range(1, m):
+        totals = totals + stats[k]
+    totals = totals / (chans * m)
+    mpb[...] = jnp.broadcast_to(totals[0:1, :], (LANES, rows)).T
+    mcb[...] = jnp.broadcast_to(totals[1:2, :], (LANES, rows)).T
+
+    def cg_block(b, _):
+        at = pl.ds(pl.multiple_of(b * BLOCK, BLOCK), BLOCK)
+        for ct in range(tiles):
+            cg[ct, at, :] = scaleb[at, :] * (
+                agrad[at, lanes(ct)] - mpb[at, :] - centered[ct, at, :] * mcb[at, :]
+            )
+        return 0
+
+    lax.fori_loop(0, blocks, cg_block, 0)
+    back_copy = pltpu.make_async_remote_copy(
+        src_ref=cg.at[:, pl.ds(0, halo), :], dst_ref=cg.at[:, pl.ds(rows, halo), :],
+        send_sem=back_sem.at[0], recv_sem=back_sem.at[1],
+        device_id={"sp": lax.rem(sp + n - 1, n)}, device_id_type=MESH,
+    )
+
+    @pl.when(sp > 0)
+    def _():
+        back_copy.start()
+
+    def side_copy(i, s):
+        return pltpu.make_async_remote_copy(
+            src_ref=zsend.at[i, s], dst_ref=zrecv.at[order[i], s],
+            send_sem=z_send.at[i, s], recv_sem=z_recv.at[order[i], s],
+            device_id={"sp": 2 * sib + par}, device_id_type=MESH,
+        )
+
+    def side_wait(p, s):
+        pltpu.make_async_remote_copy(
+            src_ref=zsend.at[0, s], dst_ref=zrecv.at[p, s],
+            send_sem=z_send.at[0, s], recv_sem=z_recv.at[p, s],
+            device_id={"sp": 2 * sib + par}, device_id_type=MESH,
+        ).wait_recv()
+
+    def cross_copy(i, s):
+        return pltpu.make_async_remote_copy(
+            src_ref=zsend.at[i, s], dst_ref=xrecv.at[s],
+            send_sem=z_send.at[i, s], recv_sem=x_recv.at[s],
+            device_id={"sp": 2 * order[i] + par}, device_id_type=MESH,
+        )
+
+    def relay(i, s):
+        p = order[i]
+        y_copy(p, s).wait_recv()
+        if i == 0:
+            zsend[i, s] = (wsum[p, s] + yrecv[p, s].astype(F32)).astype(BF16)
+            side_copy(i, s).start()
+            return
+
+        @pl.when(outer)
+        def _():
+            zsend[i, s] = (wsum[p, s] + yrecv[p, s].astype(F32)).astype(BF16)
+            side_copy(i, s).start()
+
+        @pl.when(jnp.logical_not(outer))
+        def _():
+            own = wsum[p, s] + yrecv[p, s].astype(F32)
+            side_wait(p, s)
+            zsend[i, s] = (own + zrecv[p, s].astype(F32)).astype(BF16)
+            cross_copy(i, s).start()
+
+    hear(1)
+
+    def keep_tap(k, ct, sums):
+        taploc[ct, k : k + 1, :] = jnp.sum(sums, axis=0, keepdims=True)
+
+    span = 16
+
+    def tap_tile(ct):
+        def tap_block(b, sums):
+            start = pl.multiple_of(b * span, span)
+            grad = cg[ct, pl.ds(start, span), :]
+            new = []
+            for k in range(kw):
+                prod = grad * source(gp, k + lead, ct, start, span)
+                new.append(sums[k] + jnp.sum(prod.reshape(span // 8, 8, LANES), axis=0))
+            return tuple(new)
+
+        sums = lax.fori_loop(
+            0, rows // span, tap_block, tuple(jnp.zeros((8, LANES), F32) for _ in range(kw))
+        )
+        for k in range(kw):
+            keep_tap(k, ct, sums[k])
+        keep_tap(kw, ct, gains[ct])
+
+    for ct in range(tiles):
+        tap_tile(ct)
+
+    pair_copy = pltpu.make_async_remote_copy(
+        src_ref=taploc, dst_ref=tappair, send_sem=pair_sem.at[0], recv_sem=pair_sem.at[1],
+        device_id={"sp": partner}, device_id_type=MESH,
+    )
+    pair_copy.start()
+    send(ahead, [(i, s) for i in (2, 3) for s in range(2)])
+    send(jnp.logical_not(ahead), [(i, s) for i in (1, 2, 3) for s in range(2)])
+    @pl.when(inner)
+    def _():
+        zf_relay(1)
+
+    relay(0, 0)
+    @pl.when(inner)
+    def _():
+        zf_relay(2)
+
+    relay(0, 1)
+    early = jnp.logical_and(outer, ahead)
+
+    @pl.when(early)
+    def _():
+        relay(1, 0)
+        relay(1, 1)
+
+
+    def back_block(b, _):
+        start = pl.multiple_of(b * BLOCK, BLOCK)
+        at = pl.ds(start, BLOCK)
+        for ct in range(tiles):
+            total = jnp.zeros((BLOCK, LANES), F32)
+            for k in range(kw):
+                total = total + taps[k : k + 1, lanes(ct)] * source(cg, reach - k, ct, start, BLOCK)
+            sig = jax.nn.sigmoid(gate[at, lanes(ct)].astype(F32))
+            value_grad[at, lanes(ct)] = (total * sig).astype(BF16)
+            gate_grad[at, lanes(ct)] = (
+                total * val[at, lanes(ct)].astype(F32) * sig * (1.0 - sig)
+            ).astype(BF16)
+        return 0
+
+    lax.fori_loop(0, blocks - 1, back_block, 0)
+
+    pair_copy.wait_recv()
+    tapz[q] = taploc[...] + tappair[...]
+
+    def tap_copy(k, slot):
+        return pltpu.make_async_remote_copy(
+            src_ref=tapz.at[slot], dst_ref=tapz.at[slot],
+            send_sem=tap_send.at[k], recv_sem=tap_recv.at[slot],
+            device_id={"sp": 2 * lax.rem(q + k, half) + par}, device_id_type=MESH,
+        )
+
+    @pl.loop(1, half)
+    def _(k):
+        tap_copy(k, q).start()
+
+    @pl.when(jnp.logical_not(early))
+    def _():
+        relay(1, 0)
+
+    @pl.when(jnp.logical_not(early))
+    def _():
+        relay(1, 1)
+
+    relay(2, 0)
+    @pl.when(sp < n - 1)
+    def _():
+        back_copy.wait_recv()
+
+    @pl.when(sp == n - 1)
+    def _():
+        cg[:, rows : rows + halo, :] = jnp.zeros((tiles, halo, LANES), F32)
+
+    back_block(blocks - 1, 0)
+
+    relay(2, 1)
+
+    zf_side(0, q).wait_recv()
+    zf_cross(0, q).wait_recv()
+    for k in range(2):
+        zfown[q, k] += zfside[q, k].astype(F32) + zfx[k].astype(F32)
+    zfysend[...] = zfown[q, 0].astype(BF16)
+    zf_back = pltpu.make_async_remote_copy(
+        src_ref=zfysend, dst_ref=zfyrecv, send_sem=zfy_sem.at[0], recv_sem=zfy_sem.at[1],
+        device_id={"sp": partner}, device_id_type=MESH,
+    )
+    zf_back.start()
+
+    for s in range(2):
+        y_copy(q, s).wait_recv()
+        wsum[q, s] += yrecv[q, s].astype(F32)
+    @pl.loop(1, half)
+    def _(k):
+        tap_copy(k, lax.rem(q + half - k, half)).wait_recv()
+
+    for ct in range(tiles):
+        total = tapz[0, ct]
+        for k in range(1, half):
+            total = total + tapz[k, ct]
+        taps_out[:, lanes(ct)] = total[0:kw]
+        gain_out[:, lanes(ct)] = total[kw : kw + 1]
+
+    for s in range(2):
+        side_wait(q, s)
+        pltpu.make_async_remote_copy(
+            src_ref=zsend.at[0, s], dst_ref=xrecv.at[s],
+            send_sem=z_send.at[0, s], recv_sem=x_recv.at[s],
+            device_id={"sp": partner}, device_id_type=MESH,
+        ).wait_recv()
+        whole[parts[s], :] = wsum[q, s] + zrecv[q, s].astype(F32) + xrecv[s].astype(F32)
+    zf_back.wait_recv()
+    whole[last, :] = zfown[q, 1] + zfyrecv[...].astype(F32)
+    w_out[...] = whole[...].T
+
+    @pl.when(sp < n - 1)
+    def _():
+        halo_copy.wait_send()
+
+    @pl.when(sp > 0)
+    def _():
+        back_copy.wait_send()
+
+    @pl.loop(1, m)
+    def _(k):
+        stat_copy(k, tp).wait_send()
+
+    pair_copy.wait_send()
+
+    @pl.loop(1, half)
+    def _(k):
+        tap_copy(k, q).wait_send()
+
+    for i in range(half):
+        for s in range(2):
+            y_copy(order[i], s).wait_send()
+    for i in range(half - 1):
+        for s in range(2):
+            side_copy(i, s).wait_send()
+        zf_side(i, order[i]).wait_send()
+    zf_back.wait_send()
+
+
 def finish(count, *refs):
     sem = refs[-1]
     copies = [
@@ -436,12 +979,67 @@
         copy.wait()
 
 
-def per_device(
-    n, m, glu_value, glu_gate, conv_taps, norm_gain, out_weight, norm_mean, norm_scale, out_grad
-):
-    rows, chans = glu_value.shape
-    kw = conv_taps.shape[0]
-    depth = out_grad.shape[1]
+def outputs(rows, chans, kw, dr):
+    return (
+        pltpu.VMEM((rows, chans), BF16),
+        pltpu.VMEM((rows, chans), BF16),
+        pltpu.VMEM((kw, chans), F32),
+        pltpu.VMEM((1, chans), F32),
+        pltpu.VMEM((dr, chans), F32),
+    )
+
+
+def pair_call(n, m, rows, chans, kw, depth):
+    dr = depth // n
+    half = n // 2
+    tiles = chans // LANES
+    halo = rup(kw - 1, 16)
+    taps_rows = rup(kw + 1, 8)
+    zf = chans // 4
+    cut = (chans - zf) // 2
+    vm = pltpu.VMEM
+    dma = pltpu.SemaphoreType.DMA
+    wide = vm((rows, LANES), F32)
+    block = vm((half, 2, cut, dr), BF16)
+    return pl.pallas_call(
+        functools.partial(pair_kernel, n, m, kw),
+        out_shape=outputs(rows, chans, kw, dr),
+        in_specs=[pl.BlockSpec(memory_space=pltpu.HBM)] * 8,
+        out_specs=(pl.BlockSpec(memory_space=pltpu.VMEM),) * 5,
+        scratch_shapes=[
+            vm((rows, chans), BF16), vm((rows, chans), BF16), vm((kw, chans), BF16),
+            vm((1, chans), F32), vm((1, rows), F32), vm((1, rows), F32),
+            vm((rows, depth), BF16), vm((depth, chans), BF16),
+            vm((kw, chans), F32),
+            vm((tiles, rows + halo, LANES), F32),
+            vm((tiles, rows + halo, LANES), F32),
+            vm((tiles, rows, LANES), F32),
+            vm((tiles, rows, LANES), F32),
+            vm((rows, chans), BF16),
+            vm((chans, rows), BF16),
+            vm((rows, chans), F32),
+            wide, wide, wide, wide, wide, wide,
+            vm((halo, chans), BF16), vm((halo, chans), BF16),
+            vm((m, 2, rows), F32),
+            vm((tiles, taps_rows, LANES), F32), vm((tiles, taps_rows, LANES), F32),
+            vm((half, tiles, taps_rows, LANES), F32),
+            vm((half, 2, cut, dr), F32),
+            block, block, vm((half - 1, 2, cut, dr), BF16), block, vm((2, cut, dr), BF16),
+            vm((half, 2, zf, dr), F32), vm((half - 1, 2, zf, dr), BF16), vm((half, 2, zf, dr), BF16),
+            vm((2, zf, dr), BF16), vm((zf, dr), BF16), vm((zf, dr), BF16), vm((chans, dr), F32),
+            dma((8,)), dma((2,)), dma((2,)), dma((m,)), dma((m,)), dma((2,)),
+            dma((half,)), dma((half,)),
+            dma((half, 2)), dma((half, 2)), dma((half - 1, 2)), dma((half, 2)), dma((3,)),
+            dma((half - 1,)), dma((half,)), dma((2,)),
+            pltpu.SemaphoreType.REGULAR((half - 2, 2)),
+        ],
+        compiler_params=pltpu.CompilerParams(
+            collective_id=0, has_side_effects=True, vmem_limit_bytes=VMEM_LIMIT
+        ),
+    )
+
+
+def wide_call(n, m, rows, chans, kw, depth):
     dr = depth // n
     half = n // 2
     tiles = chans // LANES
@@ -450,15 +1048,9 @@
     dma = pltpu.SemaphoreType.DMA
     whole = pl.BlockSpec(memory_space=pltpu.VMEM)
     far = pl.BlockSpec(memory_space=pltpu.HBM)
-    out = pl.pallas_call(
+    return pl.pallas_call(
         functools.partial(kernel, n, m, kw),
-        out_shape=(
-            pltpu.VMEM((rows, chans), BF16),
-            pltpu.VMEM((rows, chans), BF16),
-            pltpu.VMEM((kw, chans), F32),
-            pltpu.VMEM((1, chans), F32),
-            pltpu.VMEM((dr, chans), F32),
-        ),
+        out_shape=outputs(rows, chans, kw, dr),
         in_specs=[whole] * 6 + [far] * 2,
         out_specs=(whole,) * 5,
         scratch_shapes=[
@@ -497,11 +1089,25 @@
         compiler_params=pltpu.CompilerParams(
             collective_id=0, has_side_effects=True, vmem_limit_bytes=VMEM_LIMIT
         ),
-    )(*[
-        pltpu.with_memory_space_constraint(x, pltpu.HBM) for x in (
-        glu_value, glu_gate, conv_taps, norm_gain[None, :],
-        norm_mean[None, :], norm_scale[None, :], out_grad, out_weight,
-    )])
+    )
+
+
+def per_device(
+    n, m, glu_value, glu_gate, conv_taps, norm_gain, out_weight, norm_mean, norm_scale, out_grad
+):
+    rows, chans = glu_value.shape
+    kw = conv_taps.shape[0]
+    depth = out_grad.shape[1]
+    paired = n == 8 and (depth // n) % LANES == 0 and chans % (2 * LANES) == 0
+    call = (pair_call if paired else wide_call)(n, m, rows, chans, kw, depth)
+    out = call(*[
+        pltpu.with_memory_space_constraint(x, pltpu.HBM)
+        for x in (
+            glu_value, glu_gate, conv_taps, norm_gain[None, :],
+            norm_mean[None, :], norm_scale[None, :], out_grad, out_weight,
+        )
+    ])
+    whole = pl.BlockSpec(memory_space=pltpu.VMEM)
     out = pl.pallas_call(
         functools.partial(finish, len(out)),
         out_shape=tuple(jax.ShapeDtypeStruct(x.shape, x.dtype) for x in out),

time: 34.5 us -> 25.9 us (0.75)
  Pallas kernels: 33.7 us -> 25.1 us
    pallas_call x1, Pallas kernels: 32.8 us -> 24.2 us  [per_device(): call(*[pltpu.with_memory_space_constraint(x, pltpu.HBM) for x in (glu_val...]
where the time goes in v2:
time: 25.9 us; the launch traced here: 25.8 us
  Pallas kernels  25.1 us (97%)
  between operations  0.64 us (2%)
    pallas_call x1, Pallas kernels, per_device(): call(*[pltpu.with_memory_space_constraint(x, pltpu.HBM) for x in (glu_val...  24.2 us
    pallas_call x1, Pallas kernels, per_device(): pl.pallas_call(functools.partial(finish, len(out)), out_shape=tuple((jax....  0.94 us

profile of v2, /device:TPU:0, one launch (start us, length us, event | category | flops | bytes accessed | tf_op | source)
XLA Modules:
  0.0 25.8 jit_solution(2441949053421504121)
XLA Ops:
  0.6 24.2 %shard_map.119 = (bf16[512,256]{1,0:T(8,128)(2,1)S(1)}, bf16[512,256]{1,0:T(8,128)(2,1)S(1)}, f32[31,256]{1,0:T(8,128)S(1)}, f32[1,256]{1,0:T(1,128)S(1)}, f32[256,256]{1,0:T(8,128)S(1)}) custom-call(bf16[512,256]{1,0:T(8,128)(2,1)} %val_hbm.1, bf16[512,256]{1,0:T(8,128)(2,1)} %gate_hbm.1, bf16[31,256]{1,0:T(8,128)(2,1)} %taps_hbm.1, f32[1,256]{1,0:T(1,128)} %bitcast.6, ...), custom_call_target="tpu_custom_call" | custom-call | tf_op jit(solution)/shard_map/pallas_call | solution.py:1103
  24.8 0.9 %shard_map.120 = (bf16[512,256]{1,0:T(8,128)(2,1)}, bf16[512,256]{1,0:T(8,128)(2,1)}, f32[31,256]{1,0:T(8,128)}, f32[1,256]{1,0:T(1,128)}, f32[256,256]{1,0:T(8,128)}) custom-call(bf16[512,256]{1,0:T(8,128)(2,1)S(1)} %get-tuple-element.15.refs_0_, bf16[512,256]{1,0:T(8,128)(2,1)S(1)} %get-tuple-element.16.refs_1_, f32[31,256]{1,0:T(8,128)S(1)} %get-tuple-element.17.refs_2_, ...), custom_call_target="tpu_custom_call" | custom-call | tf_op jit(solution)/shard_map/pallas_call | solution.py:1111

commit v3 on v2

--- a/solution.py
+++ b/solution.py
@@ -430,9 +430,9 @@
     value_grad, gate_grad, taps_out, gain_out, w_out,
     val, gate, taps_in, gain, mean_row, scale_row, og, ow,
     taps, gp, cg, centered, slope, act, actt, agrad, psum, csum, meanb, scaleb, mpb, mcb,
-    halo_out, halo_in, stats, taploc, tappair, tapz, wsum, ysend, yrecv, zsend, zrecv, xrecv,
+    halo_out, halo_in, late_stats, head_stats, tapacc, taploc, tapout, tappair, tapz, wsum, ysend, yrecv, zsend, zrecv, xrecv,
     zfown, zfsend, zfside, zfx, zfysend, zfyrecv, whole,
-    load_sem, halo_sem, back_sem, stat_send, stat_recv, pair_sem, tap_send, tap_recv,
+    load_sem, halo_sem, back_sem, stat_sem, pair_sem, tap_sem,
     y_send, y_recv, z_send, z_recv, x_recv, zf_send, zf_recv, zfy_sem, hop,
 ):
     rows, chans = val.shape
@@ -513,6 +513,9 @@
         return 0
 
     lax.fori_loop(0, blocks, gate_block, 0)
+    meanb[...] = jnp.broadcast_to(mean_row[...], (LANES, rows)).T
+    scaleb[...] = jnp.broadcast_to(scale_row[...], (LANES, rows)).T
+
     near = up.astype(jnp.int32) + down.astype(jnp.int32) + has_skew.astype(jnp.int32)
     pl.semaphore_wait(barrier, m + near)
 
@@ -549,8 +552,6 @@
             pl.semaphore_wait(hop.at[r, 1], 1)
 
     tell(0)
-    meanb[...] = jnp.broadcast_to(mean_row[...], (LANES, rows)).T
-    scaleb[...] = jnp.broadcast_to(scale_row[...], (LANES, rows)).T
     def source(ref, shift, ct, start, count):
         return ref[ct, pl.ds(start + shift, count), :]
 
@@ -587,7 +588,7 @@
         agrad[at, :] = jnp.dot(og[at, :], ow[...], preferred_element_type=F32)
         return 0
 
-    lax.fori_loop(0, rows // slab, grad_block, 0)
+    lax.fori_loop(0, rows // slab, grad_block, 0, unroll=True)
 
     def stat_block(b, sums):
         at = pl.ds(pl.multiple_of(b * BLOCK, BLOCK), BLOCK)
@@ -606,9 +607,38 @@
         csum[at, :] = cross
         return tuple(new)
 
+    first = LANES // BLOCK
+
+    def pack(target, at):
+        target[tp, 0:1, :] = jnp.sum(psum[at, :].T, axis=0, keepdims=True)
+        target[tp, 1:2, :] = jnp.sum(csum[at, :].T, axis=0, keepdims=True)
+
+    def stat_copy(k, target, c):
+        return pltpu.make_async_remote_copy(
+            src_ref=target.at[tp], dst_ref=target.at[tp],
+            send_sem=stat_sem.at[c, 0], recv_sem=stat_sem.at[c, 1],
+            device_id={"tp": lax.rem(tp + k, m)}, device_id_type=MESH,
+        )
+
+    def stat_all(target, c):
+        others = target.at[pl.ds(0, m - 1)]
+        return pltpu.make_async_remote_copy(
+            src_ref=others, dst_ref=others,
+            send_sem=stat_sem.at[c, 0], recv_sem=stat_sem.at[c, 1],
+            device_id={"tp": lax.rem(tp + 1, m)}, device_id_type=MESH,
+        )
+
+    def stat_send(target, c):
+        @pl.loop(1, m)
+        def _(k):
+            stat_copy(k, target, c).start()
+
     gains = lax.fori_loop(
-        1, blocks, stat_block, tuple(jnp.zeros((8, LANES), F32) for _ in range(tiles))
-    )
+        first, blocks, stat_block, tuple(jnp.zeros((8, LANES), F32) for _ in range(tiles))
+    )
+    late_rows, head_rows = slice(LANES, rows), slice(0, LANES)
+    pack(late_stats, late_rows)
+    stat_send(late_stats, 0)
 
     hear(0)
     tell(1)
@@ -626,21 +656,6 @@
 
     conv_block(0, 0)
     turn(0)
-    gains = stat_block(0, gains)
-    stats[tp, 0:1, :] = jnp.sum(psum[...].T, axis=0, keepdims=True)
-    stats[tp, 1:2, :] = jnp.sum(csum[...].T, axis=0, keepdims=True)
-
-    def stat_copy(k, slot):
-        return pltpu.make_async_remote_copy(
-            src_ref=stats.at[slot], dst_ref=stats.at[slot],
-            send_sem=stat_send.at[k], recv_sem=stat_recv.at[slot],
-            device_id={"tp": lax.rem(tp + k, m)}, device_id_type=MESH,
-        )
-
-    @pl.loop(1, m)
-    def _(k):
-        stat_copy(k, tp).start()
-
     def piece(i):
         far = (i, i - 1)
         near_first = jnp.where(low, half - 1 - far[1], far[1]) if i else sib
@@ -658,7 +673,7 @@
     def y_copy(p, s):
         return pltpu.make_async_remote_copy(
             src_ref=ysend.at[p, s], dst_ref=yrecv.at[p, s],
-            send_sem=y_send.at[p, s], recv_sem=y_recv.at[p, s],
+            send_sem=y_send.at[0], recv_sem=y_recv.at[p, s],
             device_id={"sp": partner}, device_id_type=MESH,
         )
 
@@ -684,24 +699,23 @@
 
     def zf_copy(i, peer, target, sem):
         return pltpu.make_async_remote_copy(
-            src_ref=zfsend.at[i], dst_ref=target,
-            send_sem=zf_send.at[i], recv_sem=sem,
+            src_ref=zfsend.at[i], dst_ref=target, send_sem=zf_send.at[0], recv_sem=sem,
             device_id={"sp": 2 * peer + par}, device_id_type=MESH,
         )
 
-    def zf_side(i, p):
-        return zf_copy(i, sib, zfside.at[p], zf_recv.at[p])
+    def zf_side(i, slot):
+        return zf_copy(i, sib, zfside.at[slot], zf_recv.at[slot])
 
     def zf_cross(i, p):
         return zf_copy(i, p, zfx, x_recv.at[2])
 
     def zf_first(i):
         zfsend[i] = zfown[order[i]].astype(BF16)
-        zf_side(i, order[i]).start()
+        zf_side(i, i if i else jnp.where(outer, 0, 2)).start()
 
     def zf_relay(i):
-        zf_side(0, order[i]).wait_recv()
-        zfsend[i] = (zfown[order[i]] + zfside[order[i]].astype(F32)).astype(BF16)
+        zf_side(0, i - 1).wait_recv()
+        zfsend[i] = (zfown[order[i]] + zfside[i - 1].astype(F32)).astype(BF16)
         zf_cross(i, order[i]).start()
 
     inner = jnp.logical_not(outer)
@@ -709,6 +723,9 @@
     send(ahead, ((0, 0), (0, 1)))
     away(order[1])
     send(ahead, ((1, 0), (1, 1)))
+    gains = lax.fori_loop(0, first, stat_block, gains)
+    pack(head_stats, head_rows)
+    stat_send(head_stats, 1)
     home(order[0])
     zf_first(0)
     home(order[1])
@@ -720,24 +737,9 @@
     away(order[2])
     home(order[2])
 
-    @pl.when(outer)
-    def _():
-        zf_first(2)
-
-    send(jnp.logical_not(ahead), ((0, 0), (0, 1)))
+    send(jnp.logical_not(ahead), [(i, s) for i in (0, 1) for s in range(2)])
     away(order[3])
     home(order[3])
-
-    @pl.loop(1, m)
-    def _(k):
-        stat_copy(k, lax.rem(tp + m - k, m)).wait_recv()
-
-    totals = stats[0]
-    for k in range(1, m):
-        totals = totals + stats[k]
-    totals = totals / (chans * m)
-    mpb[...] = jnp.broadcast_to(totals[0:1, :], (LANES, rows)).T
-    mcb[...] = jnp.broadcast_to(totals[1:2, :], (LANES, rows)).T
 
     def cg_block(b, _):
         at = pl.ds(pl.multiple_of(b * BLOCK, BLOCK), BLOCK)
@@ -747,66 +749,22 @@
             )
         return 0
 
-    lax.fori_loop(0, blocks, cg_block, 0)
-    back_copy = pltpu.make_async_remote_copy(
-        src_ref=cg.at[:, pl.ds(0, halo), :], dst_ref=cg.at[:, pl.ds(rows, halo), :],
-        send_sem=back_sem.at[0], recv_sem=back_sem.at[1],
-        device_id={"sp": lax.rem(sp + n - 1, n)}, device_id_type=MESH,
-    )
-
-    @pl.when(sp > 0)
-    def _():
-        back_copy.start()
-
-    def side_copy(i, s):
-        return pltpu.make_async_remote_copy(
-            src_ref=zsend.at[i, s], dst_ref=zrecv.at[order[i], s],
-            send_sem=z_send.at[i, s], recv_sem=z_recv.at[order[i], s],
-            device_id={"sp": 2 * sib + par}, device_id_type=MESH,
-        )
-
-    def side_wait(p, s):
-        pltpu.make_async_remote_copy(
-            src_ref=zsend.at[0, s], dst_ref=zrecv.at[p, s],
-            send_sem=z_send.at[0, s], recv_sem=z_recv.at[p, s],
-            device_id={"sp": 2 * sib + par}, device_id_type=MESH,
-        ).wait_recv()
-
-    def cross_copy(i, s):
-        return pltpu.make_async_remote_copy(
-            src_ref=zsend.at[i, s], dst_ref=xrecv.at[s],
-            send_sem=z_send.at[i, s], recv_sem=x_recv.at[s],
-            device_id={"sp": 2 * order[i] + par}, device_id_type=MESH,
-        )
-
-    def relay(i, s):
-        p = order[i]
-        y_copy(p, s).wait_recv()
-        if i == 0:
-            zsend[i, s] = (wsum[p, s] + yrecv[p, s].astype(F32)).astype(BF16)
-            side_copy(i, s).start()
-            return
-
-        @pl.when(outer)
-        def _():
-            zsend[i, s] = (wsum[p, s] + yrecv[p, s].astype(F32)).astype(BF16)
-            side_copy(i, s).start()
-
-        @pl.when(jnp.logical_not(outer))
-        def _():
-            own = wsum[p, s] + yrecv[p, s].astype(F32)
-            side_wait(p, s)
-            zsend[i, s] = (own + zrecv[p, s].astype(F32)).astype(BF16)
-            cross_copy(i, s).start()
-
-    hear(1)
-
-    def keep_tap(k, ct, sums):
-        taploc[ct, k : k + 1, :] = jnp.sum(sums, axis=0, keepdims=True)
-
-    span = 16
-
-    def tap_tile(ct):
+    def cg_rows(target, c, at, begin, end):
+        stat_all(target, c).wait_recv()
+        totals = target[0]
+        for k in range(1, m):
+            totals = totals + target[k]
+        totals = totals / (chans * m)
+        count = target.shape[2]
+        mpb[at, :] = jnp.broadcast_to(totals[0:1, :], (LANES, count)).T
+        mcb[at, :] = jnp.broadcast_to(totals[1:2, :], (LANES, count)).T
+        lax.fori_loop(begin, end, cg_block, 0)
+
+    cg_rows(late_stats, 0, late_rows, first, blocks)
+
+    span = 32
+
+    def tap_rows(ct, begin, end, sums):
         def tap_block(b, sums):
             start = pl.multiple_of(b * span, span)
             grad = cg[ct, pl.ds(start, span), :]
@@ -816,39 +774,86 @@
                 new.append(sums[k] + jnp.sum(prod.reshape(span // 8, 8, LANES), axis=0))
             return tuple(new)
 
-        sums = lax.fori_loop(
-            0, rows // span, tap_block, tuple(jnp.zeros((8, LANES), F32) for _ in range(kw))
-        )
+        return lax.fori_loop(begin // span, end // span, tap_block, sums)
+
+    for ct in range(tiles):
+        sums = tap_rows(ct, LANES, rows, tuple(jnp.zeros((8, LANES), F32) for _ in range(kw)))
         for k in range(kw):
-            keep_tap(k, ct, sums[k])
-        keep_tap(kw, ct, gains[ct])
+            tapacc[ct, k] = sums[k]
+
+    def side_copy(i, slot, s):
+        return pltpu.make_async_remote_copy(
+            src_ref=zsend.at[i, s], dst_ref=zrecv.at[slot, s],
+            send_sem=z_send.at[0], recv_sem=z_recv.at[slot, s],
+            device_id={"sp": 2 * sib + par}, device_id_type=MESH,
+        )
+
+    def cross_copy(i, s):
+        return pltpu.make_async_remote_copy(
+            src_ref=zsend.at[i, s], dst_ref=xrecv.at[s],
+            send_sem=z_send.at[0], recv_sem=x_recv.at[s],
+            device_id={"sp": 2 * order[i] + par}, device_id_type=MESH,
+        )
+
+    def relay(i, s):
+        p = order[i]
+        y_copy(p, s).wait_recv()
+        if i == 0:
+            zsend[i, s] = (wsum[p, s] + yrecv[p, s].astype(F32)).astype(BF16)
+            side_copy(i, jnp.where(outer, 0, 2), s).start()
+            return
+
+        @pl.when(outer)
+        def _():
+            zsend[i, s] = (wsum[p, s] + yrecv[p, s].astype(F32)).astype(BF16)
+            side_copy(i, i, s).start()
+
+        @pl.when(inner)
+        def _():
+            own = wsum[p, s] + yrecv[p, s].astype(F32)
+            side_copy(i, i - 1, s).wait_recv()
+            zsend[i, s] = (own + zrecv[i - 1, s].astype(F32)).astype(BF16)
+            cross_copy(i, s).start()
+
+    hear(1)
+
+    @pl.when(outer)
+    def _():
+        relay(0, 0)
+
+    cg_rows(head_stats, 1, head_rows, 0, first)
+    back_copy = pltpu.make_async_remote_copy(
+        src_ref=cg.at[:, pl.ds(0, halo), :], dst_ref=cg.at[:, pl.ds(rows, halo), :],
+        send_sem=back_sem.at[0], recv_sem=back_sem.at[1],
+        device_id={"sp": lax.rem(sp + n - 1, n)}, device_id_type=MESH,
+    )
+
+    @pl.when(sp > 0)
+    def _():
+        back_copy.start()
 
     for ct in range(tiles):
-        tap_tile(ct)
-
+        sums = tap_rows(ct, 0, LANES, tuple(tapacc[ct, k] for k in range(kw)))
+        for k, total in enumerate((*sums, gains[ct])):
+            taploc[ct, k : k + 1, :] = jnp.sum(total, axis=0, keepdims=True)
+
+    tapout[...] = taploc[...].astype(BF16)
     pair_copy = pltpu.make_async_remote_copy(
-        src_ref=taploc, dst_ref=tappair, send_sem=pair_sem.at[0], recv_sem=pair_sem.at[1],
+        src_ref=tapout, dst_ref=tappair, send_sem=pair_sem.at[0], recv_sem=pair_sem.at[1],
         device_id={"sp": partner}, device_id_type=MESH,
     )
     pair_copy.start()
-    send(ahead, [(i, s) for i in (2, 3) for s in range(2)])
-    send(jnp.logical_not(ahead), [(i, s) for i in (1, 2, 3) for s in range(2)])
+    for i in (2, 3):
+        for s in range(2):
+            y_copy(order[i], s).start()
+    @pl.when(outer)
+    def _():
+        relay(0, 1)
+
     @pl.when(inner)
     def _():
         zf_relay(1)
-
-    relay(0, 0)
-    @pl.when(inner)
-    def _():
-        zf_relay(2)
-
-    relay(0, 1)
-    early = jnp.logical_and(outer, ahead)
-
-    @pl.when(early)
-    def _():
-        relay(1, 0)
-        relay(1, 1)
+        relay(0, 0)
 
 
     def back_block(b, _):
@@ -865,27 +870,42 @@
             ).astype(BF16)
         return 0
 
-    lax.fori_loop(0, blocks - 1, back_block, 0)
+    lax.fori_loop(0, blocks // 2, back_block, 0)
+
+    @pl.when(outer)
+    def _():
+        relay(1, 0)
+        relay(1, 1)
+        zf_first(2)
+
+    @pl.when(inner)
+    def _():
+        zf_relay(2)
+        relay(0, 1)
+
+    lax.fori_loop(blocks // 2, blocks - 1, back_block, 0)
 
     pair_copy.wait_recv()
-    tapz[q] = taploc[...] + tappair[...]
-
-    def tap_copy(k, slot):
+    tapz[q] = (tapout[...].astype(F32) + tappair[...].astype(F32)).astype(BF16)
+
+    def tap_copy(k, source_ref):
         return pltpu.make_async_remote_copy(
-            src_ref=tapz.at[slot], dst_ref=tapz.at[slot],
-            send_sem=tap_send.at[k], recv_sem=tap_recv.at[slot],
+            src_ref=source_ref, dst_ref=source_ref,
+            send_sem=tap_sem.at[0], recv_sem=tap_sem.at[1],
             device_id={"sp": 2 * lax.rem(q + k, half) + par}, device_id_type=MESH,
         )
 
     @pl.loop(1, half)
     def _(k):
-        tap_copy(k, q).start()
-
-    @pl.when(jnp.logical_not(early))
+        tap_copy(k, tapz.at[q]).start()
+
+    tap_all = tap_copy(1, tapz.at[pl.ds(0, half - 1)])
+
+    @pl.when(inner)
     def _():
         relay(1, 0)
 
-    @pl.when(jnp.logical_not(early))
+    @pl.when(inner)
     def _():
         relay(1, 1)
 
@@ -902,10 +922,10 @@
 
     relay(2, 1)
 
-    zf_side(0, q).wait_recv()
+    zf_side(0, 2).wait_recv()
     zf_cross(0, q).wait_recv()
     for k in range(2):
-        zfown[q, k] += zfside[q, k].astype(F32) + zfx[k].astype(F32)
+        zfown[q, k] += zfside[2, k].astype(F32) + zfx[k].astype(F32)
     zfysend[...] = zfown[q, 0].astype(BF16)
     zf_back = pltpu.make_async_remote_copy(
         src_ref=zfysend, dst_ref=zfyrecv, send_sem=zfy_sem.at[0], recv_sem=zfy_sem.at[1],
@@ -916,25 +936,19 @@
     for s in range(2):
         y_copy(q, s).wait_recv()
         wsum[q, s] += yrecv[q, s].astype(F32)
-    @pl.loop(1, half)
-    def _(k):
-        tap_copy(k, lax.rem(q + half - k, half)).wait_recv()
+    tap_all.wait_recv()
 
     for ct in range(tiles):
-        total = tapz[0, ct]
+        total = tapz[0, ct].astype(F32)
         for k in range(1, half):
-            total = total + tapz[k, ct]
+            total = total + tapz[k, ct].astype(F32)
         taps_out[:, lanes(ct)] = total[0:kw]
         gain_out[:, lanes(ct)] = total[kw : kw + 1]
 
     for s in range(2):
-        side_wait(q, s)
-        pltpu.make_async_remote_copy(
-            src_ref=zsend.at[0, s], dst_ref=xrecv.at[s],
-            send_sem=z_send.at[0, s], recv_sem=x_recv.at[s],
-            device_id={"sp": partner}, device_id_type=MESH,
-        ).wait_recv()
-        whole[parts[s], :] = wsum[q, s] + zrecv[q, s].astype(F32) + xrecv[s].astype(F32)
+        side_copy(0, 2, s).wait_recv()
+        cross_copy(0, s).wait_recv()
+        whole[parts[s], :] = wsum[q, s] + zrecv[2, s].astype(F32) + xrecv[s].astype(F32)
     zf_back.wait_recv()
     whole[last, :] = zfown[q, 1] + zfyrecv[...].astype(F32)
     w_out[...] = whole[...].T
@@ -947,23 +961,22 @@
     def _():
         back_copy.wait_send()
 
-    @pl.loop(1, m)
-    def _(k):
-        stat_copy(k, tp).wait_send()
-
+    stat_all(late_stats, 0).wait_send()
+    stat_all(head_stats, 1).wait_send()
     pair_copy.wait_send()
-
-    @pl.loop(1, half)
-    def _(k):
-        tap_copy(k, q).wait_send()
-
-    for i in range(half):
-        for s in range(2):
-            y_copy(order[i], s).wait_send()
-    for i in range(half - 1):
-        for s in range(2):
-            side_copy(i, s).wait_send()
-        zf_side(i, order[i]).wait_send()
+    tap_all.wait_send()
+    pltpu.make_async_remote_copy(
+        src_ref=ysend, dst_ref=yrecv, send_sem=y_send.at[0], recv_sem=y_recv.at[0, 0],
+        device_id={"sp": partner}, device_id_type=MESH,
+    ).wait_send()
+    pltpu.make_async_remote_copy(
+        src_ref=zsend, dst_ref=zrecv, send_sem=z_send.at[0], recv_sem=z_recv.at[0, 0],
+        device_id={"sp": partner}, device_id_type=MESH,
+    ).wait_send()
+    pltpu.make_async_remote_copy(
+        src_ref=zfsend, dst_ref=zfside, send_sem=zf_send.at[0], recv_sem=zf_recv.at[0],
+        device_id={"sp": partner}, device_id_type=MESH,
+    ).wait_send()
     zf_back.wait_send()
 
 
@@ -994,13 +1007,14 @@
     half = n // 2
     tiles = chans // LANES
     halo = rup(kw - 1, 16)
-    taps_rows = rup(kw + 1, 8)
+    taps_rows = rup(kw + 1, 16)
     zf = chans // 4
     cut = (chans - zf) // 2
     vm = pltpu.VMEM
     dma = pltpu.SemaphoreType.DMA
     wide = vm((rows, LANES), F32)
     block = vm((half, 2, cut, dr), BF16)
+    part = vm((half - 1, 2, cut, dr), BF16)
     return pl.pallas_call(
         functools.partial(pair_kernel, n, m, kw),
         out_shape=outputs(rows, chans, kw, dr),
@@ -1020,17 +1034,17 @@
             vm((rows, chans), F32),
             wide, wide, wide, wide, wide, wide,
             vm((halo, chans), BF16), vm((halo, chans), BF16),
-            vm((m, 2, rows), F32),
-            vm((tiles, taps_rows, LANES), F32), vm((tiles, taps_rows, LANES), F32),
-            vm((half, tiles, taps_rows, LANES), F32),
+            vm((m, 2, rows - LANES), F32), vm((m, 2, LANES), F32), vm((tiles, kw, 8, LANES), F32),
+            vm((tiles, taps_rows, LANES), F32), vm((tiles, taps_rows, LANES), BF16),
+            vm((tiles, taps_rows, LANES), BF16),
+            vm((half, tiles, taps_rows, LANES), BF16),
             vm((half, 2, cut, dr), F32),
-            block, block, vm((half - 1, 2, cut, dr), BF16), block, vm((2, cut, dr), BF16),
-            vm((half, 2, zf, dr), F32), vm((half - 1, 2, zf, dr), BF16), vm((half, 2, zf, dr), BF16),
+            block, block, part, part, vm((2, cut, dr), BF16),
+            vm((half, 2, zf, dr), F32), vm((half - 1, 2, zf, dr), BF16), vm((half - 1, 2, zf, dr), BF16),
             vm((2, zf, dr), BF16), vm((zf, dr), BF16), vm((zf, dr), BF16), vm((chans, dr), F32),
-            dma((8,)), dma((2,)), dma((2,)), dma((m,)), dma((m,)), dma((2,)),
-            dma((half,)), dma((half,)),
-            dma((half, 2)), dma((half, 2)), dma((half - 1, 2)), dma((half, 2)), dma((3,)),
-            dma((half - 1,)), dma((half,)), dma((2,)),
+            dma((8,)), dma((2,)), dma((2,)), dma((2, 2)), dma((2,)), dma((2,)),
+            dma((1,)), dma((half, 2)), dma((1,)), dma((half - 1, 2)), dma((3,)),
+            dma((1,)), dma((half - 1,)), dma((2,)),
             pltpu.SemaphoreType.REGULAR((half - 2, 2)),
         ],
         compiler_params=pltpu.CompilerParams(

time: 25.9 us -> 24 us (0.927)
  Pallas kernels: 25.1 us -> 23.1 us
    pallas_call x1, Pallas kernels: 24.2 us -> 22.1 us  [per_device(): call(*[pltpu.with_memory_space_constraint(x, pltpu.HBM) for x in (glu_val...]
where the time goes in v3:
time: 24 us; the launch traced here: 23.7 us
  Pallas kernels  23.1 us (96%)
  between operations  0.64 us (3%)
    pallas_call x1, Pallas kernels, per_device(): call(*[pltpu.with_memory_space_constraint(x, pltpu.HBM) for x in (glu_val...  22.1 us
    pallas_call x1, Pallas kernels, per_device(): pl.pallas_call(functools.partial(finish, len(out)), out_shape=tuple((jax....  0.94 us

profile of v3, /device:TPU:0, one launch (start us, length us, event | category | flops | bytes accessed | tf_op | source)
XLA Modules:
  0.0 23.7 jit_solution(4325164765757013435)
XLA Ops:
  0.6 22.1 %shard_map.119 = (bf16[512,256]{1,0:T(8,128)(2,1)S(1)}, bf16[512,256]{1,0:T(8,128)(2,1)S(1)}, f32[31,256]{1,0:T(8,128)S(1)}, f32[1,256]{1,0:T(1,128)S(1)}, f32[256,256]{1,0:T(8,128)S(1)}) custom-call(bf16[512,256]{1,0:T(8,128)(2,1)} %val_hbm.1, bf16[512,256]{1,0:T(8,128)(2,1)} %gate_hbm.1, bf16[31,256]{1,0:T(8,128)(2,1)} %taps_hbm.1, f32[1,256]{1,0:T(1,128)} %bitcast.6, ...), custom_call_target="tpu_custom_call" | custom-call | tf_op jit(solution)/shard_map/pallas_call | solution.py:1117
  22.8 0.9 %shard_map.120 = (bf16[512,256]{1,0:T(8,128)(2,1)}, bf16[512,256]{1,0:T(8,128)(2,1)}, f32[31,256]{1,0:T(8,128)}, f32[1,256]{1,0:T(1,128)}, f32[256,256]{1,0:T(8,128)}) custom-call(bf16[512,256]{1,0:T(8,128)(2,1)S(1)} %get-tuple-element.15.refs_0_, bf16[512,256]{1,0:T(8,128)(2,1)S(1)} %get-tuple-element.16.refs_1_, f32[31,256]{1,0:T(8,128)S(1)} %get-tuple-element.17.refs_2_, ...), custom_call_target="tpu_custom_call" | custom-call | tf_op jit(solution)/shard_map/pallas_call | solution.py:1125

commit v4 on v3

--- a/solution.py
+++ b/solution.py
@@ -424,16 +424,16 @@
         z_copy(k, lax.rem(q + k, half), q).wait_send()
 
 
-def pair_kernel(
+def pair_body(
     n, m, kw,
     val_hbm, gate_hbm, taps_hbm, gain_hbm, mean_hbm, scale_hbm, og_hbm, ow_hbm,
     value_grad, gate_grad, taps_out, gain_out, w_out,
     val, gate, taps_in, gain, mean_row, scale_row, og, ow,
     taps, gp, cg, centered, slope, act, actt, agrad, psum, csum, meanb, scaleb, mpb, mcb,
     halo_out, halo_in, late_stats, head_stats, tapacc, taploc, tapout, tappair, tapz, wsum, ysend, yrecv, zsend, zrecv, xrecv,
-    zfown, zfsend, zfside, zfx, zfysend, zfyrecv, whole,
-    load_sem, halo_sem, back_sem, stat_sem, pair_sem, tap_sem,
-    y_send, y_recv, z_send, z_recv, x_recv, zf_send, zf_recv, zfy_sem, hop,
+    zfown, zfsend, zfin, zfysend, zfyrecv, whole,
+    halo_sem, back_sem, stat_sem, pair_sem, tap_sem, y_recv, z_recv, x_recv, zf_recv, zfy_sem, hop,
+    load_sem, sent,
 ):
     rows, chans = val.shape
     tiles = chans // LANES
@@ -516,12 +516,34 @@
     meanb[...] = jnp.broadcast_to(mean_row[...], (LANES, rows)).T
     scaleb[...] = jnp.broadcast_to(scale_row[...], (LANES, rows)).T
 
+    def source(ref, shift, ct, start, count):
+        return ref[ct, pl.ds(start + shift, count), :]
+
+    def conv_rows(start, count):
+        at = pl.ds(start, count)
+        for ct in range(tiles):
+            conv = jnp.zeros((count, LANES), F32)
+            for k in range(kw):
+                conv = conv + taps[k : k + 1, lanes(ct)] * source(gp, k + lead, ct, start, count)
+            cen = (conv - meanb[at, :]) * scaleb[at, :]
+            nor = cen * gain[:, lanes(ct)]
+            sig = jax.nn.sigmoid(nor)
+            centered[ct, at, :] = cen
+            slope[ct, at, :] = sig * (1.0 + nor * (1.0 - sig))
+            act[at, lanes(ct)] = (nor * sig).astype(BF16)
+
+    def conv_block(b, _):
+        conv_rows(pl.multiple_of(b * BLOCK, BLOCK), BLOCK)
+        return 0
+
+    lax.fori_loop(1, 2, conv_block, 0)
+
     near = up.astype(jnp.int32) + down.astype(jnp.int32) + has_skew.astype(jnp.int32)
     pl.semaphore_wait(barrier, m + near)
 
     halo_copy = pltpu.make_async_remote_copy(
         src_ref=halo_out, dst_ref=halo_in,
-        send_sem=halo_sem.at[0], recv_sem=halo_sem.at[1],
+        send_sem=sent.at[0], recv_sem=halo_sem,
         device_id={"sp": lax.rem(sp + 1, n)}, device_id_type=MESH,
     )
 
@@ -552,30 +574,13 @@
             pl.semaphore_wait(hop.at[r, 1], 1)
 
     tell(0)
-    def source(ref, shift, ct, start, count):
-        return ref[ct, pl.ds(start + shift, count), :]
-
-    def conv_block(b, _):
-        start = pl.multiple_of(b * BLOCK, BLOCK)
-        at = pl.ds(start, BLOCK)
-        for ct in range(tiles):
-            conv = jnp.zeros((BLOCK, LANES), F32)
-            for k in range(kw):
-                conv = conv + taps[k : k + 1, lanes(ct)] * source(gp, k + lead, ct, start, BLOCK)
-            cen = (conv - meanb[at, :]) * scaleb[at, :]
-            nor = cen * gain[:, lanes(ct)]
-            sig = jax.nn.sigmoid(nor)
-            centered[ct, at, :] = cen
-            slope[ct, at, :] = sig * (1.0 + nor * (1.0 - sig))
-            act[at, lanes(ct)] = (nor * sig).astype(BF16)
-        return 0
-
     def turn(chunk):
         at = slice(chunk * LANES, (chunk + 1) * LANES)
         for ct in range(tiles):
             actt[lanes(ct), at] = act[at, lanes(ct)].T
 
-    lax.fori_loop(1, blocks, conv_block, 0)
+    lax.fori_loop(2, blocks, conv_block, 0)
+    conv_rows(halo, BLOCK - halo)
     for chunk in range(1, rows // LANES):
         turn(chunk)
 
@@ -616,7 +621,7 @@
     def stat_copy(k, target, c):
         return pltpu.make_async_remote_copy(
             src_ref=target.at[tp], dst_ref=target.at[tp],
-            send_sem=stat_sem.at[c, 0], recv_sem=stat_sem.at[c, 1],
+            send_sem=sent.at[2 + c], recv_sem=stat_sem.at[c],
             device_id={"tp": lax.rem(tp + k, m)}, device_id_type=MESH,
         )
 
@@ -624,7 +629,7 @@
         others = target.at[pl.ds(0, m - 1)]
         return pltpu.make_async_remote_copy(
             src_ref=others, dst_ref=others,
-            send_sem=stat_sem.at[c, 0], recv_sem=stat_sem.at[c, 1],
+            send_sem=sent.at[2 + c], recv_sem=stat_sem.at[c],
             device_id={"tp": lax.rem(tp + 1, m)}, device_id_type=MESH,
         )
 
@@ -654,15 +659,20 @@
         for ct in range(tiles):
             gp[ct, 0:halo, :] = jnp.zeros((halo, LANES), F32)
 
-    conv_block(0, 0)
+    conv_rows(0, halo)
     turn(0)
-    def piece(i):
-        far = (i, i - 1)
-        near_first = jnp.where(low, half - 1 - far[1], far[1]) if i else sib
-        far_first = jnp.where(low, half - 1 - far[0], far[0]) if i < 2 else sib
-        return jnp.where(outer, far_first, near_first)
-
-    order = [piece(0), piece(1), piece(2), q]
+    below = q == 1
+    above = q == 2
+
+    def far(i):
+        return jnp.where(low, half - 1 - i, i)
+
+    order = [
+        jnp.where(below, sib, far(0)),
+        jnp.where(below, far(0), far(1)),
+        jnp.where(below, far(1), sib),
+        q,
+    ]
     parts = (slice(0, cut), slice(cut, 2 * cut))
     last = slice(2 * cut, chans)
 
@@ -673,7 +683,7 @@
     def y_copy(p, s):
         return pltpu.make_async_remote_copy(
             src_ref=ysend.at[p, s], dst_ref=yrecv.at[p, s],
-            send_sem=y_send.at[0], recv_sem=y_recv.at[p, s],
+            send_sem=sent.at[6], recv_sem=y_recv.at[p, s],
             device_id={"sp": partner}, device_id_type=MESH,
         )
 
@@ -697,45 +707,56 @@
             for i, s in halves:
                 y_copy(order[i], s).start()
 
-    def zf_copy(i, peer, target, sem):
+    def zf_copy(i, peer, slot):
         return pltpu.make_async_remote_copy(
-            src_ref=zfsend.at[i], dst_ref=target, send_sem=zf_send.at[0], recv_sem=sem,
+            src_ref=zfsend.at[i], dst_ref=zfin.at[slot],
+            send_sem=sent.at[8], recv_sem=zf_recv.at[slot],
             device_id={"sp": 2 * peer + par}, device_id_type=MESH,
         )
 
-    def zf_side(i, slot):
-        return zf_copy(i, sib, zfside.at[slot], zf_recv.at[slot])
-
-    def zf_cross(i, p):
-        return zf_copy(i, p, zfx, x_recv.at[2])
-
-    def zf_first(i):
-        zfsend[i] = zfown[order[i]].astype(BF16)
-        zf_side(i, i if i else jnp.where(outer, 0, 2)).start()
-
-    def zf_relay(i):
-        zf_side(0, i - 1).wait_recv()
-        zfsend[i] = (zfown[order[i]] + zfside[i - 1].astype(F32)).astype(BF16)
-        zf_cross(i, order[i]).start()
+    def zf_far(i):
+        zfsend[i] = zfown[far(i)].astype(BF16)
+        zf_copy(i, far(i), jnp.where(outer, 1, 2)).start()
+
+    def zf_sib():
+        zfsend[2] = zfown[sib].astype(BF16)
+        zf_copy(2, sib, 0).start()
 
     inner = jnp.logical_not(outer)
     away(order[0])
     send(ahead, ((0, 0), (0, 1)))
-    away(order[1])
-    send(ahead, ((1, 0), (1, 1)))
     gains = lax.fori_loop(0, first, stat_block, gains)
     pack(head_stats, head_rows)
     stat_send(head_stats, 1)
+    away(order[1])
+    send(ahead, ((1, 0), (1, 1)))
+    hear(1)
     home(order[0])
-    zf_first(0)
+
+    @pl.when(jnp.logical_not(below))
+    def _():
+        zf_far(0)
+
     home(order[1])
 
-    @pl.when(outer)
-    def _():
-        zf_first(1)
+    @pl.when(below)
+    def _():
+        zf_far(0)
+
+    @pl.when(jnp.logical_not(below))
+    def _():
+        zf_far(1)
 
     away(order[2])
     home(order[2])
+
+    @pl.when(below)
+    def _():
+        zf_far(1)
+
+    @pl.when(inner)
+    def _():
+        zf_sib()
 
     send(jnp.logical_not(ahead), [(i, s) for i in (0, 1) for s in range(2)])
     away(order[3])
@@ -784,38 +805,34 @@
     def side_copy(i, slot, s):
         return pltpu.make_async_remote_copy(
             src_ref=zsend.at[i, s], dst_ref=zrecv.at[slot, s],
-            send_sem=z_send.at[0], recv_sem=z_recv.at[slot, s],
+            send_sem=sent.at[7], recv_sem=z_recv.at[slot, s],
             device_id={"sp": 2 * sib + par}, device_id_type=MESH,
         )
 
     def cross_copy(i, s):
         return pltpu.make_async_remote_copy(
             src_ref=zsend.at[i, s], dst_ref=xrecv.at[s],
-            send_sem=z_send.at[0], recv_sem=x_recv.at[s],
+            send_sem=sent.at[7], recv_sem=x_recv.at[s],
             device_id={"sp": 2 * order[i] + par}, device_id_type=MESH,
         )
 
     def relay(i, s):
         p = order[i]
+        crossing = (above, inner, below)[i]
+        slot = (jnp.where(below, 2, 0), jnp.where(below, 0, 1), jnp.where(below, 1, 2))[i]
         y_copy(p, s).wait_recv()
-        if i == 0:
-            zsend[i, s] = (wsum[p, s] + yrecv[p, s].astype(F32)).astype(BF16)
-            side_copy(i, jnp.where(outer, 0, 2), s).start()
-            return
-
-        @pl.when(outer)
+
+        @pl.when(jnp.logical_not(crossing))
         def _():
             zsend[i, s] = (wsum[p, s] + yrecv[p, s].astype(F32)).astype(BF16)
-            side_copy(i, i, s).start()
-
-        @pl.when(inner)
+            side_copy(i, slot, s).start()
+
+        @pl.when(crossing)
         def _():
             own = wsum[p, s] + yrecv[p, s].astype(F32)
-            side_copy(i, i - 1, s).wait_recv()
-            zsend[i, s] = (own + zrecv[i - 1, s].astype(F32)).astype(BF16)
+            side_copy(i, slot, s).wait_recv()
+            zsend[i, s] = (own + zrecv[slot, s].astype(F32)).astype(BF16)
             cross_copy(i, s).start()
-
-    hear(1)
 
     @pl.when(outer)
     def _():
@@ -824,7 +841,7 @@
     cg_rows(head_stats, 1, head_rows, 0, first)
     back_copy = pltpu.make_async_remote_copy(
         src_ref=cg.at[:, pl.ds(0, halo), :], dst_ref=cg.at[:, pl.ds(rows, halo), :],
-        send_sem=back_sem.at[0], recv_sem=back_sem.at[1],
+        send_sem=sent.at[1], recv_sem=back_sem,
         device_id={"sp": lax.rem(sp + n - 1, n)}, device_id_type=MESH,
     )
 
@@ -839,7 +856,7 @@
 
     tapout[...] = taploc[...].astype(BF16)
     pair_copy = pltpu.make_async_remote_copy(
-        src_ref=tapout, dst_ref=tappair, send_sem=pair_sem.at[0], recv_sem=pair_sem.at[1],
+        src_ref=tapout, dst_ref=tappair, send_sem=sent.at[4], recv_sem=pair_sem,
         device_id={"sp": partner}, device_id_type=MESH,
     )
     pair_copy.start()
@@ -850,9 +867,8 @@
     def _():
         relay(0, 1)
 
-    @pl.when(inner)
-    def _():
-        zf_relay(1)
+    @pl.when(below)
+    def _():
         relay(0, 0)
 
 
@@ -876,11 +892,10 @@
     def _():
         relay(1, 0)
         relay(1, 1)
-        zf_first(2)
-
-    @pl.when(inner)
-    def _():
-        zf_relay(2)
+        zf_sib()
+
+    @pl.when(below)
+    def _():
         relay(0, 1)
 
     lax.fori_loop(blocks // 2, blocks - 1, back_block, 0)
@@ -891,7 +906,7 @@
     def tap_copy(k, source_ref):
         return pltpu.make_async_remote_copy(
             src_ref=source_ref, dst_ref=source_ref,
-            send_sem=tap_sem.at[0], recv_sem=tap_sem.at[1],
+            send_sem=sent.at[5], recv_sem=tap_sem,
             device_id={"sp": 2 * lax.rem(q + k, half) + par}, device_id_type=MESH,
         )
 
@@ -900,6 +915,11 @@
         tap_copy(k, tapz.at[q]).start()
 
     tap_all = tap_copy(1, tapz.at[pl.ds(0, half - 1)])
+
+    @pl.when(above)
+    def _():
+        relay(0, 0)
+        relay(0, 1)
 
     @pl.when(inner)
     def _():
@@ -922,13 +942,15 @@
 
     relay(2, 1)
 
-    zf_side(0, 2).wait_recv()
-    zf_cross(0, q).wait_recv()
+    for slot in range(half - 1):
+        zf_copy(0, sib, slot).wait_recv()
     for k in range(2):
-        zfown[q, k] += zfside[2, k].astype(F32) + zfx[k].astype(F32)
+        zfown[q, k] += (
+            zfin[0, k].astype(F32) + zfin[1, k].astype(F32) + zfin[2, k].astype(F32)
+        )
     zfysend[...] = zfown[q, 0].astype(BF16)
     zf_back = pltpu.make_async_remote_copy(
-        src_ref=zfysend, dst_ref=zfyrecv, send_sem=zfy_sem.at[0], recv_sem=zfy_sem.at[1],
+        src_ref=zfysend, dst_ref=zfyrecv, send_sem=sent.at[9], recv_sem=zfy_sem,
         device_id={"sp": partner}, device_id_type=MESH,
     )
     zf_back.start()
@@ -966,15 +988,15 @@
     pair_copy.wait_send()
     tap_all.wait_send()
     pltpu.make_async_remote_copy(
-        src_ref=ysend, dst_ref=yrecv, send_sem=y_send.at[0], recv_sem=y_recv.at[0, 0],
+        src_ref=ysend, dst_ref=yrecv, send_sem=sent.at[6], recv_sem=y_recv.at[0, 0],
         device_id={"sp": partner}, device_id_type=MESH,
     ).wait_send()
     pltpu.make_async_remote_copy(
-        src_ref=zsend, dst_ref=zrecv, send_sem=z_send.at[0], recv_sem=z_recv.at[0, 0],
+        src_ref=zsend, dst_ref=zrecv, send_sem=sent.at[7], recv_sem=z_recv.at[0, 0],
         device_id={"sp": partner}, device_id_type=MESH,
     ).wait_send()
     pltpu.make_async_remote_copy(
-        src_ref=zfsend, dst_ref=zfside, send_sem=zf_send.at[0], recv_sem=zf_recv.at[0],
+        src_ref=zfsend, dst_ref=zfin, send_sem=sent.at[8], recv_sem=zf_recv.at[0],
         device_id={"sp": partner}, device_id_type=MESH,
     ).wait_send()
     zf_back.wait_send()
@@ -990,6 +1012,13 @@
         copy.start()
     for copy in copies:
         copy.wait()
+
+
+def pair_kernel(n, m, kw, *refs):
+    pl.run_scoped(
+        functools.partial(pair_body, n, m, kw, *refs),
+        pltpu.SemaphoreType.DMA((8,)), pltpu.SemaphoreType.DMA((10,)),
+    )
 
 
 def outputs(rows, chans, kw, dr):
@@ -1041,10 +1070,9 @@
             vm((half, 2, cut, dr), F32),
             block, block, part, part, vm((2, cut, dr), BF16),
             vm((half, 2, zf, dr), F32), vm((half - 1, 2, zf, dr), BF16), vm((half - 1, 2, zf, dr), BF16),
-            vm((2, zf, dr), BF16), vm((zf, dr), BF16), vm((zf, dr), BF16), vm((chans, dr), F32),
-            dma((8,)), dma((2,)), dma((2,)), dma((2, 2)), dma((2,)), dma((2,)),
-            dma((1,)), dma((half, 2)), dma((1,)), dma((half - 1, 2)), dma((3,)),
-            dma((1,)), dma((half - 1,)), dma((2,)),
+            vm((zf, dr), BF16), vm((zf, dr), BF16), vm((chans, dr), F32),
+            dma, dma, dma((2,)), dma, dma, dma((half, 2)), dma((half - 1, 2)), dma((2,)),
+            dma((half - 1,)), dma,
             pltpu.SemaphoreType.REGULAR((half - 2, 2)),
         ],
         compiler_params=pltpu.CompilerParams(

time: 24 us -> 23.6 us (0.983)
  Pallas kernels: 23.1 us -> 22.6 us
    pallas_call x1, Pallas kernels: 22.1 us -> 21.6 us  [per_device(): call(*[pltpu.with_memory_space_constraint(x, pltpu.HBM) for x in (glu_val...]
where the time goes in v4:
time: 23.6 us; the launch traced here: 23.2 us
  Pallas kernels  22.6 us (96%)
  between operations  0.64 us (3%)
    pallas_call x1, Pallas kernels, per_device(): call(*[pltpu.with_memory_space_constraint(x, pltpu.HBM) for x in (glu_val...  21.6 us
    pallas_call x1, Pallas kernels, per_device(): pl.pallas_call(functools.partial(finish, len(out)), out_shape=tuple((jax....  0.94 us

profile of v4, /device:TPU:0, one launch (start us, length us, event | category | flops | bytes accessed | tf_op | source)
XLA Modules:
  0.0 23.2 jit_solution(8616004104252875708)
XLA Ops:
  0.6 21.6 %shard_map.119 = (bf16[512,256]{1,0:T(8,128)(2,1)S(1)}, bf16[512,256]{1,0:T(8,128)(2,1)S(1)}, f32[31,256]{1,0:T(8,128)S(1)}, f32[1,256]{1,0:T(1,128)S(1)}, f32[256,256]{1,0:T(8,128)S(1)}) custom-call(bf16[512,256]{1,0:T(8,128)(2,1)} %refs_0_.1, bf16[512,256]{1,0:T(8,128)(2,1)} %refs_1_.1, bf16[31,256]{1,0:T(8,128)(2,1)} %refs_2_.1, f32[1,256]{1,0:T(1,128)} %bitcast.6, ...), custom_call_target="tpu_custom_call" | custom-call | tf_op jit(solution)/shard_map/pallas_call | solution.py:1145
  22.3 0.9 %shard_map.120 = (bf16[512,256]{1,0:T(8,128)(2,1)}, bf16[512,256]{1,0:T(8,128)(2,1)}, f32[31,256]{1,0:T(8,128)}, f32[1,256]{1,0:T(1,128)}, f32[256,256]{1,0:T(8,128)}) custom-call(bf16[512,256]{1,0:T(8,128)(2,1)S(1)} %get-tuple-element.15.refs_0_, bf16[512,256]{1,0:T(8,128)(2,1)S(1)} %get-tuple-element.16.refs_1_, f32[31,256]{1,0:T(8,128)S(1)} %get-tuple-element.17.refs_2_, ...), custom_call_target="tpu_custom_call" | custom-call | tf_op jit(solution)/shard_map/pallas_call | solution.py:1153
